TPU v7x, 128 devices: a whole 4x4x4 slice. The times are simulated.
128 devices in a mesh: sp: 16 (over z, x), fs: 4 (over y), tp: 2 (over core).
Axes of the slice: x: 4, y: 4, z: 4, core: 2. Of those that a mesh axis runs over, the one named last changes fastest.
Arguments:
- tokens: bfloat16 [49152, 2048], P(('fs', 'sp'), 'tp'), parts along dimension 0, may hold values from -6 to 6
- norm_gain: bfloat16 [2048], replicated, may hold values from 0.099609375 to 1.8984375
- w_query: bfloat16 [2048, 1024], P(None, 'tp'), may hold values from -0.125 to 0.125
- w_key: bfloat16 [2048, 1024], P(None, 'tp'), may hold values from -0.125 to 0.125
- w_value: bfloat16 [2048, 1024], P(None, 'tp'), may hold values from -0.125 to 0.125
- log_decay: float32 [8, 12288], P('tp', 'sp'), may hold values from -1 to 0
- w_conv_in: bfloat16 [2048, 1024], P(None, 'tp'), may hold values from -0.125 to 0.125
- w_conv_pre: bfloat16 [2048, 1024], P(None, 'tp'), may hold values from -0.125 to 0.125
- w_conv_post: bfloat16 [2048, 1024], P(None, 'tp'), may hold values from -0.125 to 0.125
- conv_taps: bfloat16 [3, 1024], P(None, 'tp'), may hold values from -3 to 3
- w_out_ret: bfloat16 [1024, 2048], replicated, may hold values from -0.125 to 0.125
- w_out_conv: bfloat16 [1024, 2048], replicated, may hold values from -0.125 to 0.125
Outputs:
- mixed: bfloat16 [49152, 2048], P(('fs', 'sp', 'tp')), parts along dimension 0
There are 4 independent parts, one for each index of `fs`. A program takes and returns all parts, laid end to end along the dimension named above; an argument that names none is the same for every part. Nothing has to cross between parts.
All inputs are finite; a program needn't handle non-finite values.
Results may differ from a plain program's by a relative error of at most 0.012.
Values may be sent and summed in bfloat16 or wider, within the bound.
A program may use at most 128 MiB of HBM per device.

v0:
```python
import jax
import jax.numpy as jnp
from jax import lax
from jax.sharding import PartitionSpec as P

DH = 128
TAPS = 3
SPAN = 128


epsilon = 1e-06


def shifted(value, axis, steps):
    count = lax.axis_size(axis)
    first, last = (max(0, -steps), min(count, count - steps))
    return lax.ppermute(value, axis, [(source, source + steps) for source in range(first, last)])


def copy_for_each(shard, axis):
    devices = lax.axis_size(axis)
    return lax.all_to_all(
        jnp.broadcast_to(shard[None], (devices, *shard.shape)), axis, 0, 0, tiled=True
    )


def joined_by_halves(pieces, combine):
    while len(jax.tree.leaves(pieces)[0]) > 1:
        pieces = jax.vmap(combine)(
            *(jax.tree.map(lambda part: part[side::2], pieces) for side in (0, 1))
        )
    return jax.tree.map(lambda part: part[0], pieces)


def entering(shard, axis, combine, identity):
    devices, place = (lax.axis_size(axis), lax.axis_index(axis))
    passed = jnp.arange(devices) < place

    def kept(part, zero, own):
        part = jnp.where(
            passed.reshape(-1, *(1 for _ in own.shape)),
            part.astype(own.dtype),
            jnp.asarray(zero, own.dtype),
        )
        return part

    pieces = jax.tree.map(
        lambda part: copy_for_each(part, axis),
        jax.tree.map(lambda part, kind: part.astype(kind), shard, (jnp.bfloat16, jnp.bfloat16)),
    )
    return joined_by_halves(jax.tree.map(kept, pieces, identity, shard), combine)


def split_up(shard, dim, devices):
    before, after = (shard.shape[:dim], shard.shape[dim + 1 :])
    return jnp.moveaxis(shard.reshape(*before, devices, -1, *after), dim, 0)


def summed_on_arrival(shard, axis, dim):
    tiles = split_up(shard, dim, lax.axis_size(axis))
    arrived = lax.all_to_all(tiles, axis, split_axis=0, concat_axis=0, tiled=True)
    return arrived.astype(jnp.float32).sum(axis=0)


def rotate(vectors, positions):
    halfway = vectors.shape[-1] // 2
    inverse = 10000.0 ** (-jnp.arange(halfway, dtype=jnp.float32) / halfway)
    angles = positions.astype(jnp.float32)[:, None] * inverse[None, :]
    cosines = jnp.cos(angles)[:, None, :]
    sinusoid = jnp.sin(angles)[:, None, :]
    leading = vectors[..., :halfway]
    trailing = vectors[..., halfway:]
    return jnp.concatenate(
        [leading * cosines - trailing * sinusoid, leading * sinusoid + trailing * cosines], axis=-1
    )


def combine_states(earlier, later):
    return (earlier[0] * later[0], later[0][:, None, None] * earlier[1] + later[1])


def body(
    tokens,
    norm_gain,
    w_query,
    w_key,
    w_value,
    log_decay,
    w_conv_in,
    w_conv_pre,
    w_conv_post,
    conv_taps,
    w_out_ret,
    w_out_conv,
):
    gathered = lax.all_gather(tokens, "tp", axis=1, tiled=True)
    floats = gathered.astype(jnp.float32)
    normed = (
        floats
        * lax.rsqrt(jnp.mean(floats * floats, axis=-1, keepdims=True) + epsilon)
        * norm_gain.astype(jnp.float32)
    ).astype(jnp.bfloat16)
    tok_rows = normed.shape[0]
    head_count = w_query.shape[1] // DH
    positions = lax.axis_index("sp") * tok_rows + jnp.arange(tok_rows, dtype=jnp.int32)

    def project(weight):
        return jnp.dot(normed, weight, preferred_element_type=jnp.float32)

    queries = rotate(project(w_query).reshape(tok_rows, head_count, DH), positions).astype(
        jnp.bfloat16
    )
    keys_turned = (
        rotate(project(w_key).reshape(tok_rows, head_count, DH), positions) * DH ** (-0.5)
    ).astype(jnp.bfloat16)
    values = project(w_value).astype(jnp.bfloat16).reshape(tok_rows, head_count, DH)
    conv_in = lax.optimization_barrier(project(w_conv_in).astype(jnp.bfloat16))
    conv_pre = lax.optimization_barrier(project(w_conv_pre).astype(jnp.bfloat16))
    conv_post = lax.optimization_barrier(project(w_conv_post).astype(jnp.bfloat16))
    gated_in = (conv_pre.astype(jnp.float32) * conv_in.astype(jnp.float32)).astype(jnp.bfloat16)
    rim_rows = shifted(gated_in[tok_rows - (TAPS - 1) :], "sp", 1)
    extended = jnp.concatenate([rim_rows, gated_in], axis=0)
    convolved = jnp.zeros(gated_in.shape, jnp.float32)
    for tap_index in range(TAPS):
        convolved = convolved + conv_taps[tap_index].astype(jnp.float32) * extended[
            tap_index : tap_index + tok_rows
        ].astype(jnp.float32)
    conv_out = (conv_post.astype(jnp.float32) * convolved).astype(jnp.bfloat16)
    blocks = tok_rows // SPAN
    query_blocks = queries.reshape(blocks, SPAN, head_count, DH)
    key_blocks = keys_turned.reshape(blocks, SPAN, head_count, DH)
    value_blocks = values.reshape(blocks, SPAN, head_count, DH)
    cumulative = jnp.cumsum(log_decay.reshape(head_count, blocks, SPAN), axis=-1).transpose(1, 0, 2)
    lower_mask = jnp.tril(jnp.ones((SPAN, SPAN), bool))
    differences = cumulative[..., :, None] - cumulative[..., None, :]
    decay_weights = jnp.where(lower_mask, jnp.exp(jnp.minimum(differences, 0.0)), 0.0)
    scores = jnp.einsum(
        "bshd,bthd->bhst", query_blocks, key_blocks, preferred_element_type=jnp.float32
    )
    mix_weights = (scores * decay_weights).astype(jnp.bfloat16)
    inside = jnp.einsum(
        "bhst,bthd->bshd", mix_weights, value_blocks, preferred_element_type=jnp.float32
    )
    block_ends = cumulative[..., -1]
    tail_decay = jnp.exp(block_ends[..., None] - cumulative)
    weighted = value_blocks.astype(jnp.float32) * tail_decay.transpose(0, 2, 1)[..., None]
    block_states = jnp.einsum(
        "bshd,bshe->bhde", key_blocks.astype(jnp.float32), weighted, precision=lax.Precision.HIGHEST
    )

    def advance(carried, inputs):
        end_decay, fresh_state = inputs
        return (jnp.exp(end_decay)[:, None, None] * carried + fresh_state, carried)

    empty_state = jnp.zeros((head_count, DH, DH), jnp.float32)
    local_total, local_starts = lax.scan(advance, empty_state, (block_ends, block_states))
    decay_total = jnp.exp(jnp.sum(block_ends, axis=0))
    unused_decay, incoming = entering(
        (decay_total, local_total),
        "sp",
        combine_states,
        (jnp.ones_like(decay_total), jnp.zeros_like(local_total)),
    )
    prefix_ends = jnp.cumsum(block_ends, axis=0) - block_ends
    starts = local_starts + jnp.exp(prefix_ends)[..., None, None] * incoming[None]
    across = jnp.einsum(
        "bshd,bhde->bshe", query_blocks.astype(jnp.float32), starts, precision=lax.Precision.HIGHEST
    )
    retained = inside + jnp.exp(cumulative).transpose(0, 2, 1)[..., None] * across
    normalized = retained * lax.rsqrt(
        jnp.mean(retained * retained, axis=-1, keepdims=True) + epsilon
    )
    ret_out = normalized.astype(jnp.bfloat16).reshape(tok_rows, head_count * DH)
    ret_width = ret_out.shape[1]
    conv_width = conv_out.shape[1]
    pair_index = lax.axis_index("tp")
    ret_rows = lax.dynamic_slice_in_dim(w_out_ret, pair_index * ret_width, ret_width, 0)
    conv_rows = lax.dynamic_slice_in_dim(w_out_conv, pair_index * conv_width, conv_width, 0)
    mixed_rows = summed_on_arrival(
        (
            jnp.dot(ret_out, ret_rows, preferred_element_type=jnp.float32)
            + jnp.dot(conv_out, conv_rows, preferred_element_type=jnp.float32)
        ).astype(jnp.bfloat16),
        "tp",
        0,
    )
    return mixed_rows.astype(jnp.bfloat16)


def solution(mesh):
    in_specs = (
        P(("fs", "sp"), "tp"),
        P(),
        P(None, "tp"),
        P(None, "tp"),
        P(None, "tp"),
        P("tp", "sp"),
        P(None, "tp"),
        P(None, "tp"),
        P(None, "tp"),
        P(None, "tp"),
        P(),
        P(),
    )
    out_specs = P(("fs", "sp", "tp"), None)
    return jax.shard_map(body, mesh=mesh, in_specs=in_specs, out_specs=out_specs, check_vma=False)
```

profile of v0, /device:TPU:1, one launch (start us, length us, event | category | flops | bytes accessed | tf_op | source)
XLA Modules:
  0.0 131.2 jit_solution(18343770314797849168)
XLA Ops:
  9.9 8.4 %all-to-all-start = ((bf16[16,1,4]{2,1,0:T(2,128)(2,1)}), bf16[16,1,4]{2,1,0:T(2,128)(2,1)S(1)}, u32[]{:S(2)}, u32[]{:S(2)}) async-start(bf16[16,1,4]{2,1,0:T(2,128)(2,1)} %broadcast_in_dim.35), calls=%async_computation | async-start | bytes 16384 | tf_op jit(solution)/shard_map/all_to_all | solution.py:22
  28.1 2.7 %fusion.2 = f32[768]{0:T(1024)S(1)} fusion(bf16[768,2048]{1,0:T(8,128)(2,1)} %all-gather.2.cloned.1.call-done), kind=kLoop, calls=%fused_computation.7 | loop fusion | flops 4717824 | bytes 3148800 | tf_op jit(solution)/shard_map/reduce_sum | solution.py:100
  31.4 1.8 %convolution_convert_fusion.3 = bf16[768,512]{1,0:T(8,128)(2,1)S(1)} fusion(bf16[2048,512]{1,0:T(8,128)(2,1)S(1)} %copy-done, bf16[768,2048]{1,0:T(8,128)(2,1)S(1)} %copy-done.2, f32[2048]{0:T(1024)S(1)} %copy-done.18, f32[768]{0:T(1024)S(1)} %add_rsqrt_fusion.1), kind=kOutput, calls=%fused_computation.34 | convolution fusion | flops 1617297408 | bytes 6040576 | tf_op jit(solution)/shard_map/dot_general | solution.py:108
  34.4 4.7 %fusion.49 = f32[768,512]{0,1:T(8,128)S(1)} fusion(bf16[2048,512]{1,0:T(8,128)(2,1)} %param.16, bf16[768,2048]{1,0:T(8,128)(2,1)} %all-gather.2.cloned.1.call-done, f32[2048]{0:T(1024)} %convert_element_type.101, f32[768]{0:T(1024)} %copy-done.21), kind=kOutput, calls=%fused_computation.92 | convolution fusion | flops 1616904192 | bytes 6827008 | tf_op jit(solution)/shard_map/dot_general | solution.py:108
  39.1 2.0 %fusion.47 = f32[768,512]{0,1:T(8,128)S(1)} fusion(bf16[2048,512]{1,0:T(8,128)(2,1)S(1)} %copy-done.31, bf16[768,2048]{1,0:T(8,128)(2,1)S(1)} %copy-done.3, f32[2048]{0:T(1024)S(1)} %copy-done.19, f32[768]{0:T(1024)S(1)} %copy-done.22), kind=kOutput, calls=%fused_computation.91 | convolution fusion | flops 1616904192 | bytes 6827008 | tf_op jit(solution)/shard_map/dot_general | solution.py:108
  44.5 1.7 %copy.63 = f32[6,128,4,64]{3,1,2,0:T(8,128)} copy(f32[6,128,4,64]{1,0,3,2:T(8,128)S(1)} %concatenate.23) | data formatting | bytes 1572864 | tf_op jit(solution)/shard_map/concatenate | solution.py:73
  46.2 2.0 %fusion.8 = bf16[6,128,4,128]{3,1,2,0:T(8,128)(2,1)S(1)} fusion(f32[6,128,4,64]{3,1,2,0:T(8,128)S(1)} %copy.64, f32[6,128,4,64]{3,1,2,0:T(8,128)} %copy.63), kind=kLoop, calls=%fused_computation.17 | loop fusion | flops 1179648 | bytes 2359296 | tf_op jit(solution)/shard_map/convert_element_type | solution.py:115
  50.5 9.2 %while.14 = (s32[]{:T(128)}, f32[4,128,128]{2,1,0:T(8,128)S(1)}, f32[6,4,128,128]{3,2,1,0:T(8,128)}, f32[6,4]{1,0:T(8,128)}, f32[6,4,128,128]{3,2,1,0:T(8,128)S(1)}) while((s32[]{:T(128)}, f32[4,128,128]{2,1,0:T(8,128)S(1)}, f32[6,4,128,128]{3,2,1,0:T(8,128)}, f32[6,4]{1,0:T(8,128)}, ...), condition=%wide.region_3.4_spmd.clone.clone, body=%wide.region_2.3_spmd.clone.sunk.clone | while | flops 262147 | bytes 1310860 | solution.py:156
  59.7 1.9 %broadcast_in_dim.38 = bf16[16,4,128,128]{3,2,1,0:T(8,128)(2,1)} broadcast(bf16[4,128,128]{2,1,0:T(8,128)(2,1)S(1)} %convert_element_type.111), dimensions={1,2,3} | broadcast | bytes 2228224 | tf_op jit(solution)/shard_map/broadcast_in_dim | solution.py:23
  61.6 6.7 %all-to-all-start.1 = ((bf16[16,4,128,128]{3,2,1,0:T(8,128)(2,1)}), bf16[16,4,128,128]{3,2,1,0:T(8,128)(2,1)S(1)}, u32[]{:S(2)}, u32[]{:S(2)}) async-start(bf16[16,4,128,128]{3,2,1,0:T(8,128)(2,1)} %broadcast_in_dim.38), calls=%async_computation.1 | async-start | bytes 4194304 | tf_op jit(solution)/shard_map/all_to_all | solution.py:22
  68.3 5.4 %convolution_convert_fusion.2 = bf16[768,512]{1,0:T(8,128)(2,1)} fusion(bf16[2048,512]{1,0:T(8,128)(2,1)} %param.22, bf16[768,2048]{1,0:T(8,128)(2,1)} %all-gather.2.cloned.1.call-done, f32[2048]{0:T(1024)S(1)} %copy-done.19, f32[768]{0:T(1024)S(1)} %copy-done.22), kind=kOutput, calls=%fused_computation.33 | convolution fusion | flops 1617297408 | bytes 6040576 | tf_op jit(solution)/shard_map/dot_general | solution.py:108
  73.7 1.8 %convolution_convert_fusion.1 = bf16[768,512]{1,0:T(8,128)(2,1)S(1)} fusion(bf16[2048,512]{1,0:T(8,128)(2,1)S(1)} %copy-done.32, bf16[768,2048]{1,0:T(8,128)(2,1)S(1)} %copy-done.4, f32[2048]{0:T(1024)S(1)} %copy-done.19, f32[768]{0:T(1024)S(1)} %copy-done.22), kind=kOutput, calls=%fused_computation.32 | convolution fusion | flops 1617297408 | bytes 6040576 | tf_op jit(solution)/shard_map/dot_general | solution.py:108
  75.6 1.8 %convolution_convert_fusion = bf16[768,512]{1,0:T(8,128)(2,1)S(1)} fusion(bf16[2048,512]{1,0:T(8,128)(2,1)S(1)} %copy-done.33, bf16[768,2048]{1,0:T(8,128)(2,1)S(1)} %copy-done.4, f32[2048]{0:T(1024)S(1)} %copy-done.19, f32[768]{0:T(1024)S(1)} %copy-done.22), kind=kOutput, calls=%fused_computation.31 | convolution fusion | flops 1617297408 | bytes 6040576 | tf_op jit(solution)/shard_map/dot_general | solution.py:108
  79.1 3.8 %collective-permute-start = (bf16[2,512]{1,0:T(2,128)(2,1)}, bf16[2,512]{1,0:T(2,128)(2,1)}, u32[]{:S(2)}, u32[]{:S(2)}) collective-permute-start(bf16[2,512]{1,0:T(2,128)(2,1)} %slice.114), channel_id=1, source_target_pairs={{0,8},{8,16},{16,24},{24,32},{32,40},{40,48},{48,56},{56,64},{64,7... | collective-permute-start | bytes 6152 | tf_op jit(solution)/shard_map/ppermute | solution.py:17
  83.0 2.3 %concatenate.20 = bf16[6,128,4,64]{1,0,3,2:T(8,128)(2,1)} reshape(bf16[768,4,64]{0,2,1:T(8,128)(2,1)} %get-tuple-element.85) | data formatting | bytes 786432 | tf_op jit(solution)/shard_map/concatenate | solution.py:73
  85.2 2.3 %copy.61 = bf16[6,128,4,64]{3,1,2,0:T(8,128)(2,1)} copy(bf16[6,128,4,64]{1,0,3,2:T(8,128)(2,1)} %concatenate.20) | data formatting | bytes 786432 | tf_op jit(solution)/shard_map/concatenate | solution.py:73
  88.8 2.3 %copy.62 = bf16[6,128,4,64]{3,1,2,0:T(8,128)(2,1)} copy(bf16[6,128,4,64]{1,0,3,2:T(8,128)(2,1)} %concatenate.21) | data formatting | bytes 786432 | tf_op jit(solution)/shard_map/concatenate | solution.py:73
  91.1 4.0 %fusion.18 = f32[6,4,128,128]{3,2,1,0:T(8,128)} fusion(bf16[6,128,4,128]{3,1,2,0:T(8,128)(2,1)} %copy-done.8, f32[6,4,128]{2,1,0:T(4,128)S(1)} %copy-done.17, pred[128,128]{1,0:T(8,128)(4,1)S(1)} %copy-done.15, bf16[6,128,4,128]{3,2,1,0:T(4,128)(2,1)S(1)} %copy-done.5, bf16[6,128,4,64]{3,1,2,0:T(8,128)(2,1)} %copy.62, bf16[6,128,4,64]{3,1,2,0:T(8,128)(2,1)} %copy.61), kind=kOutput, calls=%fused_computation.35 | convolution fusion | flops 204865536 | bytes 3960832 | tf_op jit(solution)/shard_map/bhst,bthd->bshd/dot_general | solution.py:141
  95.1 2.1 %all-to-all-done.1 = bf16[16,4,128,128]{3,2,1,0:T(8,128)(2,1)S(1)} async-done(((bf16[16,4,128,128]{3,2,1,0:T(8,128)(2,1)}), bf16[16,4,128,128]{3,2,1,0:T(8,128)(2,1)S(1)}, u32[]{:S(2)}, u32[]{:S(2)}) %all-to-all-start.1) | async-done | bytes 2097184 | tf_op jit(solution)/shard_map/all_to_all | solution.py:22
  100.9 1.8 %multiply_reduce_fusion = (f32[6,128,4]{1,2,0:T(4,128)S(1)}, f32[6,128,4,128]{1,3,2,0:T(8,128)S(1)}) fusion(bf16[6,128,4,64]{3,1,2,0:T(8,128)(2,1)S(1)} %copy-done.7, bf16[6,128,4,64]{3,1,2,0:T(8,128)(2,1)S(1)} %copy-done.6, f32[6,4,128,128]{3,2,1,0:T(8,128)S(1)} %copy-done.10, f32[4,128,128]{2,1,0:T(8,128)S(1)} %fusion.35, f32[6,4]{1,0:T(8,128)S(1)} %copy.73, ...), kind=kOutput, calls=%fused_computation.23 | convolution fusion | flops 607908864 | bytes 5791840 | tf_op jit(solution)/shard_map/bshd,bhde->bshe/dot_general | solution.py:166
  103.7 3.5 %fusion.6 = f32[768,2048]{1,0:T(8,128)S(1)} fusion(bf16[1024,2048]{1,0:T(8,128)(2,1)} %param.24, s32[]{:T(128)S(6)} %select_n.21, bf16[96,8,4,128]{3,2,1,0:T(4,128)(2,1)S(1)} %bitcast.59), kind=kOutput, calls=%fused_computation.13 | convolution fusion | flops 1610612736 | bytes 9175044 | tf_op jit(solution)/shard_map/dot_general | solution.py:181
  107.3 3.0 %add_convert_fusion = bf16[768,2048]{1,0:T(8,128)(2,1)S(1)} fusion(f32[768,2048]{1,0:T(8,128)S(1)} %fusion.6, bf16[1024,2048]{1,0:T(8,128)(2,1)S(1)} %copy-done.30, s32[]{:T(128)S(6)} %select_n.21, bf16[768,512]{1,0:T(8,128)(2,1)S(1)} %copy-done.13, bf16[768,512]{1,0:T(8,128)(2,1)S(1)} %copy-done.34, bf16[2,512]{1,0:T(2,128)(2,1)} %collective-permute-done, ...), kind=kOutput, calls=%fused_computation.10 | convolution fusion | flops 1620443136 | bytes 13115396 | tf_op jit(solution)/shard_map/dot_general | solution.py:182
  110.2 9.9 %all_to_all.16 = bf16[2,384,2048]{2,1,0:T(8,128)(2,1)} all-to-all(bf16[2,384,2048]{2,1,0:T(8,128)(2,1)S(1)} %bitcast.60), channel_id=1, replica_groups=mesh['sp'=16,'fs'=4,'tp'=2] {'tp'}, dimensions={0} | all-to-all | bytes 6291456 | tf_op jit(solution)/shard_map/all_to_all | solution.py:61
  120.1 4.2 %reduce_sum.42 = bf16[384,2048]{1,0:T(8,128)(2,1)} reduce(bf16[2,384,2048]{2,1,0:T(8,128)(2,1)} %all_to_all.16, bf16[]{:T(256)} %constant.61.clone.1), dimensions={0}, to_apply=%region_7.8 | reduce | flops 786432 | bytes 4718594 | tf_op jit(solution)/shard_map/reduce_sum | solution.py:62
  (149 shorter events, 36.9 us)
Async XLA Ops:
  6.5 24.9 %copy-start = (bf16[2048,512]{1,0:T(8,128)(2,1)S(1)}, bf16[2048,512]{1,0:T(8,128)(2,1)}, u32[]{:S(2)}) copy-start(bf16[2048,512]{1,0:T(8,128)(2,1)} %param.18) | copy-start | bytes 6291460
  6.5 21.5 %all-gather.2.cloned.1.call-start = ((), (), s32[]{:S(2)}) async-start(), calls=%async_computation.3 | async-start | bytes 4718592 | tf_op jit(solution)/shard_map/all_gather | solution.py:96
  9.9 14.8 %all-to-all-start = ((bf16[16,1,4]{2,1,0:T(2,128)(2,1)}), bf16[16,1,4]{2,1,0:T(2,128)(2,1)S(1)}, u32[]{:S(2)}, u32[]{:S(2)}) async-start(bf16[16,1,4]{2,1,0:T(2,128)(2,1)} %broadcast_in_dim.35), calls=%async_computation | async-start | bytes 16384 | tf_op jit(solution)/shard_map/all_to_all | solution.py:22
  21.9 8.9 %copy-start.24 = (pred[16]{0:T(512)(128)(4,1)}, pred[16]{0:T(512)(128)(4,1)S(1)}, u32[]{:S(2)}) copy-start(pred[16]{0:T(512)(128)(4,1)S(1)} %iota_compare_fusion.1) | copy-start | bytes 52
  28.1 3.3 %copy-start.18 = (f32[2048]{0:T(1024)S(1)}, f32[2048]{0:T(1024)}, u32[]{:S(2)}) copy-start(f32[2048]{0:T(1024)} %convert_element_type.101) | copy-start | bytes 24580
  34.4 4.7 %copy-start.3 = (bf16[768,2048]{1,0:T(8,128)(2,1)S(1)}, bf16[768,2048]{1,0:T(8,128)(2,1)}, u32[]{:S(2)}) copy-start(bf16[768,2048]{1,0:T(8,128)(2,1)} %all-gather.2.cloned.1.call-done) | copy-start | bytes 9437188
  34.4 4.7 %copy-start.19 = (f32[2048]{0:T(1024)S(1)}, f32[2048]{0:T(1024)}, u32[]{:S(2)}) copy-start(f32[2048]{0:T(1024)} %convert_element_type.101) | copy-start | bytes 24580
  34.4 4.7 %copy-start.22 = (f32[768]{0:T(1024)S(1)}, f32[768]{0:T(1024)}, u32[]{:S(2)}) copy-start(f32[768]{0:T(1024)} %copy-done.21) | copy-start | bytes 9220
  34.4 4.8 %copy-start.31 = (bf16[2048,512]{1,0:T(8,128)(2,1)S(1)}, bf16[2048,512]{1,0:T(8,128)(2,1)}, u32[]{:S(2)}) copy-start(bf16[2048,512]{1,0:T(8,128)(2,1)} %param.17) | copy-start | bytes 6291460
  61.6 35.7 %all-to-all-start.1 = ((bf16[16,4,128,128]{3,2,1,0:T(8,128)(2,1)}), bf16[16,4,128,128]{3,2,1,0:T(8,128)(2,1)S(1)}, u32[]{:S(2)}, u32[]{:S(2)}) async-start(bf16[16,4,128,128]{3,2,1,0:T(8,128)(2,1)} %broadcast_in_dim.38), calls=%async_computation.1 | async-start | bytes 4194304 | tf_op jit(solution)/shard_map/all_to_all | solution.py:22
  68.3 5.4 %copy-start.4 = (bf16[768,2048]{1,0:T(8,128)(2,1)S(1)}, bf16[768,2048]{1,0:T(8,128)(2,1)}, u32[]{:S(2)}) copy-start(bf16[768,2048]{1,0:T(8,128)(2,1)} %all-gather.2.cloned.1.call-done) | copy-start | bytes 9437188
  68.3 5.4 %copy-start.32 = (bf16[2048,512]{1,0:T(8,128)(2,1)S(1)}, bf16[2048,512]{1,0:T(8,128)(2,1)}, u32[]{:S(2)}) copy-start(bf16[2048,512]{1,0:T(8,128)(2,1)} %param.21) | copy-start | bytes 6291460
  77.4 10.1 %copy-start.9 = (bf16[768,4,64]{0,2,1:T(8,128)(2,1)S(1)}, bf16[768,4,64]{0,2,1:T(8,128)(2,1)}, u32[]{:S(2)}) copy-start(bf16[768,4,64]{0,2,1:T(8,128)(2,1)} %get-tuple-element.86) | copy-start | bytes 1179652
  79.1 28.1 %collective-permute-start = (bf16[2,512]{1,0:T(2,128)(2,1)}, bf16[2,512]{1,0:T(2,128)(2,1)}, u32[]{:S(2)}, u32[]{:S(2)}) collective-permute-start(bf16[2,512]{1,0:T(2,128)(2,1)} %slice.114), channel_id=1, source_target_pairs={{0,8},{8,16},{16,24},{24,32},{32,40},{40,48},{48,56},{56,64},{64,7... | collective-permute-start | bytes 6152 | tf_op jit(solution)/shard_map/ppermute | solution.py:17
  82.9 8.1 %copy-start.15 = (pred[128,128]{1,0:T(8,128)(4,1)S(1)}, pred[128,128]{1,0:T(8,128)(4,1)}, u32[]{:S(2)}) copy-start(pred[128,128]{1,0:T(8,128)(4,1)} %iota_compare_fusion) | copy-start | bytes 49156
  83.0 8.1 %copy-start.17 = (f32[6,4,128]{2,1,0:T(4,128)S(1)}, f32[6,4,128]{2,1,0:T(4,128)}, u32[]{:S(2)}) copy-start(f32[6,4,128]{2,1,0:T(4,128)} %copy.65) | copy-start | bytes 36868
  91.1 6.2 %copy-start.25 = (pred[16]{0:T(512)(128)(4,1)S(1)}, pred[16]{0:T(512)(128)(4,1)}, u32[]{:S(2)}) copy-start(pred[16]{0:T(512)(128)(4,1)} %copy-done.24) | copy-start | bytes 52
  103.6 3.6 %copy-start.13 = (bf16[768,512]{1,0:T(8,128)(2,1)S(1)}, bf16[768,512]{1,0:T(8,128)(2,1)}, u32[]{:S(2)}) copy-start(bf16[768,512]{1,0:T(8,128)(2,1)} %copy-done.12) | copy-start | bytes 2359300
  103.6 3.6 %copy-start.26 = (f32[1,512]{1,0:T(1,128)S(1)}, f32[1,512]{1,0:T(1,128)}, u32[]{:S(2)}) copy-start(f32[1,512]{1,0:T(1,128)} %get-tuple-element.95) | copy-start | bytes 6148
  103.6 3.6 %copy-start.27 = (f32[1,512]{1,0:T(1,128)S(1)}, f32[1,512]{1,0:T(1,128)}, u32[]{:S(2)}) copy-start(f32[1,512]{1,0:T(1,128)} %get-tuple-element.96) | copy-start | bytes 6148
  103.6 3.6 %copy-start.28 = (f32[1,512]{1,0:T(1,128)S(1)}, f32[1,512]{1,0:T(1,128)}, u32[]{:S(2)}) copy-start(f32[1,512]{1,0:T(1,128)} %get-tuple-element.97) | copy-start | bytes 6148
  103.6 3.6 %copy-start.30 = (bf16[1024,2048]{1,0:T(8,128)(2,1)S(1)}, bf16[1024,2048]{1,0:T(8,128)(2,1)}, u32[]{:S(2)}) copy-start(bf16[1024,2048]{1,0:T(8,128)(2,1)} %param.25) | copy-start | bytes 12582916
  103.7 3.6 %copy-start.34 = (bf16[768,512]{1,0:T(8,128)(2,1)S(1)}, bf16[768,512]{1,0:T(8,128)(2,1)}, u32[]{:S(2)}) copy-start(bf16[768,512]{1,0:T(8,128)(2,1)} %convolution_convert_fusion.2) | copy-start | bytes 2359300
  110.2 14.1 %copy-start.1 = (bf16[2048,512]{1,0:T(8,128)(2,1)S(1)}, bf16[2048,512]{1,0:T(8,128)(2,1)}, u32[]{:S(2)}) copy-start(bf16[2048,512]{1,0:T(8,128)(2,1)} %param.18) | copy-start | bytes 6291460
  (15 other events, 24.8 us)
Sparse Core Ops, SparseCore 0:
  9.0 18.4 all-gather.1
where the time goes:
time: 132 us; the launch traced here: 131 us
  matrix products  31.5 us (24%)
  local copies, waits for them, and re-layouts  31.4 us (24%)
  other arithmetic  22.6 us (17%)
  starting transfers between devices  18.9 us (14%)
  between operations  13.9 us (11%)
  blocking collectives  9.89 us (7%)
  waiting for transfers between devices  2.86 us (2%)
    dot_general x6, matrix products, project(): return jnp.dot(normed, weight, preferred_element_type=jnp.float32)  17.7 us
    all_to_all x2, starting transfers between devices, copy_for_each(): lax.all_to_all(jnp.broadcast_to(shard[None], (devices, *shard.shape)), ax...  15.1 us
    concatenate x8, local copies, waits for them, and re-layouts, rotate(): jnp.concatenate([leading * cosines - trailing * sinusoid, leading * sinus...  11.7 us
    all_to_all x1, blocking collectives, summed_on_arrival(): lax.all_to_all(tiles, axis, split_axis=0, concat_axis=0, tiled=True)  9.89 us
    unnamed x71, local copies, waits for them, and re-layouts  5.45 us
    dynamic_update_slice x6, other arithmetic, body(): lax.scan(advance, empty_state, (block_ends, block_states))  4.36 us
    reduce_sum x1, other arithmetic, summed_on_arrival(): return arrived.astype(jnp.float32).sum(axis=0)  4.21 us
    exp x6, local copies, waits for them, and re-layouts, advance(): return (jnp.exp(end_decay)[:, None, None] * carried + fresh_state, carried)  4.12 us
  transfers between devices with their start and end apart: 4, of which 1 were waited for; matrix products, arithmetic and copies ran while one was open for 32% of the time, Pallas kernels for 0%

commit v1 on v0

v1 whole, which is shorter than its diff:
```python
import functools

import jax
import jax.numpy as jnp
import numpy as np
from jax import lax
from jax.experimental import pallas as pl
from jax.experimental.pallas import tpu as pltpu
from jax.sharding import PartitionSpec as P

DH = 128
SPAN = 128
ROWS = 768
HALF = 384
BLOCKS = 6
HEADS = 4
KW = 1024
NW = 512
D = 2048
EPS = 1e-06
KEY_SCALE = 128.0 ** -0.5
F32 = jnp.float32
BF16 = jnp.bfloat16
MESH = pl.DeviceIdType.MESH
WEIGHTS = ("wk", "wv", "wq", "wci", "wcp", "wcq")


def rotation_tables(places):
    half = DH // 2
    rate = 10000.0 ** (-np.arange(half, dtype=np.float64) / half)
    inner = np.arange(SPAN, dtype=np.float64)[:, None] * rate[None, :]
    inner = np.concatenate([inner, inner], axis=1)
    sign = np.concatenate([-np.ones(half), np.ones(half)])[None, :]
    within = np.stack(
        [np.cos(inner), np.sin(inner), sign * np.cos(inner), sign * np.sin(inner)]
    ).astype(np.float32)
    start = np.arange(places * BLOCKS, dtype=np.float64) * SPAN
    outer = start[:, None] * rate[None, :]
    outer = np.concatenate([outer, outer], axis=1).reshape(places, BLOCKS, DH)
    bases = np.zeros((places, 16, DH), np.float32)
    bases[:, :BLOCKS] = np.cos(outer)
    bases[:, 8 : 8 + BLOCKS] = np.sin(outer)
    return within, bases


def mm(a, b):
    return jnp.dot(a, b, preferred_element_type=F32)


def kernel(
    tok, gain, ld, taps, wk, wv, wq, wci, wcp, wcq, woc, wor, tabs, bases,
    out,
    xo, go, gp, wbuf, wob, acc, kb, vb, qb, cib, postb, gbuf, cob, cor,
    retb, retr, inside, states, starts, oacc, ssb, pack, pack_far, rot_c, rot_s,
    tabv, basev, gainv, ldv, tapv, ldp, cumr, colrep, lrow, lcol,
    a1, a2, b1, b2, bm, pre,
    sem_tok, sem_small, sem_w, sem_wo,
    ts, tr, l1s, l1r, l2s, l2r, a1s, a1r, a2s, a2r, b1s, b1r, b2s, b2r,
    hs, hr, cs, cr, rs, rr, ps, pr,
):
    sp = lax.axis_index("sp")
    tp = lax.axis_index("tp")
    x = lax.rem(sp, 4)
    z = lax.div(sp, 4)
    other = 1 - tp
    row_peer = [z * 4 + lax.rem(x + k, 4) for k in (1, 2, 3)]
    col_peer = [lax.rem(z + k, 4) * 4 + x for k in (1, 2, 3)]
    after = lax.rem(sp + 1, 16)
    before = lax.rem(sp + 15, 16)

    barrier = pltpu.get_barrier_semaphore()
    pl.semaphore_signal(barrier, inc=1, device_id={"tp": other}, device_id_type=MESH)
    for peer in row_peer + col_peer + [after, before]:
        pl.semaphore_signal(barrier, inc=1, device_id={"sp": peer}, device_id_type=MESH)

    def remote(src, dst, send, recv, where):
        return pltpu.make_async_remote_copy(
            src_ref=src, dst_ref=dst, send_sem=send, recv_sem=recv,
            device_id=where, device_id_type=MESH,
        )

    own_k = pl.multiple_of(tp * KW, KW)
    far_k = pl.multiple_of(other * KW, KW)
    own_n = pl.multiple_of(tp * NW, NW)
    far_n = pl.multiple_of(other * NW, NW)
    own_rows = pl.ds(pl.multiple_of(tp * HALF, HALF), HALF)
    far_rows = pl.ds(pl.multiple_of(other * HALF, HALF), HALF)

    tok_load = [
        pltpu.make_async_copy(
            tok.at[pl.ds(c * 256, 256), :], xo.at[pl.ds(c * 256, 256), :], sem_tok.at[c]
        )
        for c in range(3)
    ]
    small = [
        pltpu.make_async_copy(ld, ldv, sem_small.at[0]),
        pltpu.make_async_copy(gain, gainv, sem_small.at[1]),
        pltpu.make_async_copy(taps, tapv, sem_small.at[2]),
        pltpu.make_async_copy(tabs, tabv, sem_small.at[3]),
        pltpu.make_async_copy(bases.at[sp], basev, sem_small.at[4]),
    ]
    hbm = dict(zip(WEIGHTS, (wk, wv, wq, wci, wcp, wcq)))
    index = {name: i for i, name in enumerate(WEIGHTS)}

    def w_load(name, part):
        i = index[name]
        rows = pl.ds(own_k if part == 0 else far_k, KW)
        return pltpu.make_async_copy(
            hbm[name].at[rows, :], wbuf.at[i, part], sem_w.at[i * 2 + part]
        )

    def wo_load(i, part):
        rows = pl.ds(own_n if part == 0 else far_n, NW)
        return pltpu.make_async_copy(
            (woc, wor)[i].at[rows, :], wob.at[i, part], sem_wo.at[i * 2 + part]
        )

    small[0].start()
    small[1].start()
    for copy in tok_load:
        copy.start()
    w_load("wk", 0).start()
    w_load("wv", 0).start()
    small[4].start()
    small[3].start()
    small[2].start()

    ldp[...] = jnp.zeros_like(ldp)
    small[0].wait()
    for b in range(BLOCKS):
        ldp[b * 8 : b * 8 + HEADS, :] = ldv[:, b * SPAN : (b + 1) * SPAN]
    upper = (
        lax.broadcasted_iota(jnp.int32, (SPAN, SPAN), 0)
        <= lax.broadcasted_iota(jnp.int32, (SPAN, SPAN), 1)
    )
    ones = jnp.where(upper, 1.0, 0.0).astype(BF16)
    rest = ldp[...]
    total = jnp.zeros((SPAN, SPAN), F32)
    for _ in range(3):
        piece = rest.astype(BF16)
        total = total + mm(piece, ones)
        rest = rest - piece.astype(F32)
    cumr[...] = total
    columns = total.T
    for b in range(BLOCKS):
        for h in range(HEADS):
            i = b * 8 + h
            colrep[b, h] = jnp.broadcast_to(columns[:, i : i + 1], (SPAN, SPAN))

    def block_end(b, h):
        return colrep[b, h, SPAN - 1 : SPAN, :]

    lrow[x] = jnp.zeros((8, SPAN), F32)
    for h in range(HEADS):
        whole = block_end(0, h)
        for b in range(1, BLOCKS):
            whole = whole + block_end(b, h)
        lrow[x, h : h + 1, :] = whole

    lane = lax.broadcasted_iota(jnp.int32, (SPAN, SPAN), 1)
    packed = jnp.zeros((SPAN, SPAN), F32)
    for i in range(BLOCKS):
        if i % 2 == 0:
            tok_load[i // 2].wait()
        rows = slice(i * 128, i * 128 + 128)
        value = xo[rows, :].astype(F32)
        squares = jnp.sum(value * value, axis=1, keepdims=True)
        spread = jnp.broadcast_to(squares, (SPAN, SPAN))
        ssb[rows, :] = spread
        packed = jnp.where(lane == i, spread, packed)
    pack[...] = packed

    pl.semaphore_wait(barrier, 9)
    pack_send = remote(pack, pack_far, ps, pr, {"tp": other})
    pack_send.start()
    l1_send = [
        remote(lrow.at[x], lrow.at[x], l1s.at[k], l1r.at[k], {"sp": row_peer[k]})
        for k in range(3)
    ]
    for copy in l1_send:
        copy.start()
    w_load("wq", 0).start()
    w_load("wci", 0).start()

    small[1].wait()
    small[3].wait()
    small[4].wait()

    def tables(b, carry):
        rows = pl.ds(pl.multiple_of(b * 128, 128), 128)
        base_c = basev[pl.ds(b, 1), :]
        base_s = basev[pl.ds(b + 8, 1), :]
        rot_c[rows, :] = base_c * tabv[0] - base_s * tabv[1]
        rot_s[rows, :] = base_s * tabv[2] + base_c * tabv[3]
        return carry

    lax.fori_loop(0, BLOCKS, tables, 0)
    weight = gainv[:, pl.ds(own_k, KW)].astype(F32)
    pack_send.wait_recv()
    tok_send = [
        remote(
            go.at[pl.ds(c * 256, 256), :], gp.at[pl.ds(c * 256, 256), :],
            ts.at[c], tr.at[c], {"tp": other},
        )
        for c in range(3)
    ]
    for i in range(BLOCKS):
        rows = slice(i * 128, i * 128 + 128)
        level = ssb[rows, :] + jnp.broadcast_to(pack_far[:, i : i + 1], (SPAN, SPAN))
        scale = lax.rsqrt(level * (1.0 / D) + EPS)
        for c in range(KW // 128):
            at = slice(c * 128, c * 128 + 128)
            go[rows, at] = (xo[rows, at].astype(F32) * scale * weight[:, at]).astype(BF16)
        if i in (2, 4):
            tok_send[i // 2 - 1].start()
    tok_send[2].start()

    def near_product(name):
        i = index[name]
        w_load(name, 0).wait()

        def step(n, carry):
            cols = pl.ds(pl.multiple_of(n * 256, 256), 256)
            acc[i, :, cols] = mm(go[...], wbuf[i, 0, :, cols])
            return carry

        lax.fori_loop(0, 2, step, 0)

    near_product("wk")
    w_load("wk", 1).start()
    w_load("wv", 1).start()
    near_product("wv")
    w_load("wq", 1).start()
    w_load("wci", 1).start()
    near_product("wq")
    w_load("wcp", 0).start()
    w_load("wcp", 1).start()
    near_product("wci")
    w_load("wcq", 0).start()
    w_load("wcq", 1).start()

    for copy in l1_send:
        copy.wait_recv()
    line = [lrow[i] for i in range(4)]

    def between(low, high):
        parts = [
            jnp.where(jnp.logical_and(i > low, i < high), line[i], 0.0) for i in range(4)
        ]
        return (parts[0] + parts[1]) + (parts[2] + parts[3])

    row_total = (line[0] + line[1]) + (line[2] + line[3])
    lcol[z, 0] = row_total
    lcol[z, 1] = between(x, 4)
    l2_send = [
        remote(lcol.at[z], lcol.at[z], l2s.at[k], l2r.at[k], {"sp": col_peer[k]})
        for k in range(3)
    ]
    for copy in l2_send:
        copy.start()

    for copy in tok_send:
        copy.wait_recv()

    def rotated(value):
        return value * rot_c[...] + pltpu.roll(value, 64, axis=1) * rot_s[...]

    exchange = []
    for n in range(2):
        cols = slice(n * 256, n * 256 + 256)
        if n == 0:
            w_load("wk", 1).wait()
        kk = acc[0, :, cols] + mm(gp[...], wbuf[0, 1, :, cols])
        for j in range(2):
            at = slice(n * 256 + j * 128, n * 256 + j * 128 + 128)
            kb[:, at] = (rotated(kk[:, j * 128 : j * 128 + 128]) * KEY_SCALE).astype(BF16)
        if n == 0:
            w_load("wv", 1).wait()
        vv = acc[1, :, cols] + mm(gp[...], wbuf[1, 1, :, cols])
        for j in range(2):
            at = slice(n * 256 + j * 128, n * 256 + j * 128 + 128)
            vb[:, at] = vv[:, j * 128 : j * 128 + 128].astype(BF16)
        slot = a1.at[x] if n == 0 else b1.at[z]
        for j in range(2):
            h = n * 2 + j
            at = slice(h * 128, h * 128 + 128)
            whole = None
            for b in range(BLOCKS):
                rows = slice(b * 128, b * 128 + 128)
                end = block_end(b, h)
                tail = jnp.exp(end - colrep[b, h])
                weighted = (vb[rows, at].astype(F32) * tail).astype(BF16)
                fresh = lax.dot_general(
                    kb[rows, at], weighted, (((0,), (0,)), ((), ())),
                    preferred_element_type=F32,
                )
                states[b, h] = fresh
                whole = fresh if whole is None else jnp.exp(end) * whole + fresh
            slot[j] = whole.astype(BF16)
        for k in range(3):
            if n == 0:
                copy = remote(a1.at[x], a1.at[x], a1s.at[k], a1r.at[k], {"sp": row_peer[k]})
            else:
                copy = remote(b1.at[z], b1.at[z], b1s.at[k], b1r.at[k], {"sp": col_peer[k]})
            copy.start()
            exchange.append(copy)

    w_load("wq", 1).wait()

    def query_step(n, carry):
        cols = pl.ds(pl.multiple_of(n * 256, 256), 256)
        qq = acc[2, :, cols] + mm(gp[...], wbuf[2, 1, :, cols])
        for j in range(2):
            at = pl.ds(pl.multiple_of(n * 256 + j * 128, 128), 128)
            qb[:, at] = rotated(qq[:, j * 128 : j * 128 + 128]).astype(BF16)
        return carry

    lax.fori_loop(0, 2, query_step, 0)

    w_load("wci", 1).wait()

    def conv_in_step(n, carry):
        cols = pl.ds(pl.multiple_of(n * 256, 256), 256)
        value = acc[3, :, cols] + mm(gp[...], wbuf[3, 1, :, cols])
        cib[:, cols] = value.astype(BF16)
        return carry

    lax.fori_loop(0, 2, conv_in_step, 0)

    w_load("wcp", 0).wait()
    w_load("wcp", 1).wait()
    for i in range(2):
        for part in range(2):
            wo_load(i, part).start()

    def conv_pre_step(n, carry):
        cols = pl.ds(pl.multiple_of(n * 256, 256), 256)
        value = mm(go[...], wbuf[4, 0, :, cols]) + mm(gp[...], wbuf[4, 1, :, cols])
        pre_gate = value.astype(BF16).astype(F32)
        gated = (pre_gate * cib[:, cols].astype(F32)).astype(BF16).astype(F32)
        for j in range(2):
            gbuf[n * 2 + j, 8 : 8 + ROWS, :] = gated[:, j * 128 : j * 128 + 128]
        return carry

    lax.fori_loop(0, 2, conv_pre_step, 0)
    halo = remote(
        gbuf.at[:, pl.ds(ROWS, 8), :], gbuf.at[:, pl.ds(0, 8), :], hs, hr, {"sp": after}
    )
    halo.start()

    for copy in l2_send:
        copy.wait_recv()
    row_sums = [lcol[i, 0] for i in range(4)]
    suffix = [lcol[i, 1] for i in range(4)]
    before_me = between(-1, x)

    def rows_between(low):
        parts = [
            jnp.where(jnp.logical_and(i > low, i < z), row_sums[i], 0.0) for i in range(4)
        ]
        return (parts[0] + parts[1]) + (parts[2] + parts[3])

    def lane_row(weight, h):
        return weight[h : h + 1, :]

    to_end = [jnp.exp(between(i, 4)) for i in range(4)]
    to_me = [jnp.where(i < x, jnp.exp(between(i, x)), 0.0) for i in range(4)]
    for k in range(3):
        exchange[k].wait_recv()
    for j in range(2):
        parts = [a1[i, j].astype(F32) for i in range(4)]
        row_state = lane_row(to_end[0], j) * parts[0]
        prefix = lane_row(to_me[0], j) * parts[0]
        for i in range(1, 4):
            row_state = row_state + lane_row(to_end[i], j) * parts[i]
            prefix = prefix + lane_row(to_me[i], j) * parts[i]
        pre[j] = prefix
        a2[z, j] = row_state.astype(BF16)
    second = []
    for k in range(3):
        copy = remote(a2.at[z], a2.at[z], a2s.at[k], a2r.at[k], {"sp": col_peer[k]})
        copy.start()
        second.append(copy)
    above = [
        jnp.where(i < z, jnp.exp(suffix[i] + rows_between(i)), 0.0) for i in range(4)
    ]
    for k in range(3):
        exchange[3 + k].wait_recv()
    e_own = jnp.exp(before_me)
    for j in range(2):
        h = 2 + j
        column = lane_row(above[0], h) * b1[0, j].astype(F32)
        for i in range(1, 4):
            column = column + lane_row(above[i], h) * b1[i, j].astype(F32)
        mine = b1[z, j].astype(F32)
        b2[x, j] = (lane_row(e_own, h) * column).astype(BF16)
        for k in range(3):
            target = lax.rem(x + k + 1, 4)
            e_col = jnp.exp(between(-1, target))
            e_mine = jnp.where(x < target, jnp.exp(between(x, target)), 0.0)
            bm[k, j] = (lane_row(e_col, h) * column + lane_row(e_mine, h) * mine).astype(BF16)
    for k in range(3):
        copy = remote(bm.at[k], b2.at[x], b2s.at[k], b2r.at[k], {"sp": row_peer[k]})
        copy.start()
        second.append(copy)

    w_load("wcq", 0).wait()
    w_load("wcq", 1).wait()

    def conv_post_step(n, carry):
        cols = pl.ds(pl.multiple_of(n * 256, 256), 256)
        value = mm(go[...], wbuf[5, 0, :, cols]) + mm(gp[...], wbuf[5, 1, :, cols])
        postb[:, cols] = value.astype(BF16)
        return carry

    lax.fori_loop(0, 2, conv_post_step, 0)

    small[2].wait()
    halo.wait_recv()

    @pl.when(sp == 0)
    def _():
        gbuf[:, 0:8, :] = jnp.zeros((4, 8, 128), F32)

    for c in range(4):
        at = slice(c * 128, c * 128 + 128)
        summed = jnp.zeros((ROWS, 128), F32)
        for i in range(3):
            summed = summed + tapv[i : i + 1, at].astype(F32) * gbuf[c, 6 + i : 6 + i + ROWS, :]
        cob[:, at] = (postb[:, at].astype(F32) * summed).astype(BF16)
    conv_send = remote(cob.at[far_rows, :], cor, cs, cr, {"tp": other})
    conv_send.start()

    lower = (
        lax.broadcasted_iota(jnp.int32, (SPAN, SPAN), 0)
        >= lax.broadcasted_iota(jnp.int32, (SPAN, SPAN), 1)
    )

    def inside_step(b, carry):
        rows = pl.ds(pl.multiple_of(b * 128, 128), 128)
        for h in range(HEADS):
            at = slice(h * 128, h * 128 + 128)
            gap = colrep[b, h] - cumr[pl.ds(b * 8 + h, 1), :]
            weight = jnp.where(lower, jnp.exp(jnp.minimum(gap, 0.0)), 0.0)
            scores = lax.dot_general(
                qb[rows, at], kb[rows, at], (((1,), (1,)), ((), ())),
                preferred_element_type=F32,
            )
            mixed = (scores * weight).astype(BF16)
            inside[rows, at] = mm(mixed, vb[rows, at])
        return carry

    lax.fori_loop(0, BLOCKS, inside_step, 0)

    conv_send.wait_recv()
    for i in range(2):
        for part in range(2):
            wo_load(i, part).wait()

    def out_conv_step(n, carry):
        cols = pl.ds(pl.multiple_of(n * 512, 512), 512)
        oacc[:, cols] = mm(cob[own_rows, :], wob[0, 0, :, cols]) + mm(
            cor[...], wob[0, 1, :, cols]
        )
        return carry

    lax.fori_loop(0, 4, out_conv_step, 0)

    for k in range(6):
        second[k].wait_recv()
    down = [
        jnp.where(i < z, jnp.exp(rows_between(i) + before_me), 0.0) for i in range(4)
    ]
    for h in range(HEADS):
        j = h % 2
        if h < 2:
            state = pre[j]
            for i in range(4):
                state = state + lane_row(down[i], h) * a2[i, j].astype(F32)
        else:
            state = b2[0, j].astype(F32)
            for i in range(1, 4):
                state = state + b2[i, j].astype(F32)
        for b in range(BLOCKS):
            starts[b, h] = state.astype(BF16)
            if b < BLOCKS - 1:
                state = jnp.exp(block_end(b, h)) * state + states[b, h]

    def across(first):
        def step(i, carry):
            b = first + i
            rows = pl.ds(pl.multiple_of(b * 128, 128), 128)
            for h in range(HEADS):
                at = slice(h * 128, h * 128 + 128)
                value = inside[rows, at] + jnp.exp(colrep[b, h]) * mm(
                    qb[rows, at], starts[b, h]
                )
                level = jnp.mean(value * value, axis=1, keepdims=True)
                retb[rows, at] = (value * lax.rsqrt(level + EPS)).astype(BF16)
            return carry

        lax.fori_loop(0, 3, step, 0)

    across(other * 3)
    ret_send = remote(retb.at[far_rows, :], retr, rs, rr, {"tp": other})
    ret_send.start()
    across(tp * 3)

    def out_near_step(n, carry):
        cols = pl.ds(pl.multiple_of(n * 512, 512), 512)
        oacc[:, cols] += mm(retb[own_rows, :], wob[1, 0, :, cols])
        return carry

    lax.fori_loop(0, 4, out_near_step, 0)
    ret_send.wait_recv()

    def out_far_step(n, carry):
        cols = pl.ds(pl.multiple_of(n * 512, 512), 512)
        out[:, cols] = (oacc[:, cols] + mm(retr[...], wob[1, 1, :, cols])).astype(BF16)
        return carry

    lax.fori_loop(0, 4, out_far_step, 0)

    for copy in [pack_send] + tok_send + l1_send + l2_send + exchange + second + [halo, conv_send, ret_send]:
        copy.wait_send()


def body(
    tokens, norm_gain, w_query, w_key, w_value, log_decay, w_conv_in, w_conv_pre,
    w_conv_post, conv_taps, w_out_ret, w_out_conv,
):
    within, bases = rotation_tables(16)
    dma = pltpu.SemaphoreType.DMA
    v = pltpu.VMEM
    scratch = [
        v((ROWS, KW), BF16), v((ROWS, KW), BF16), v((ROWS, KW), BF16),
        v((6, 2, KW, NW), BF16), v((2, 2, NW, D), BF16), v((4, ROWS, NW), F32),
        v((ROWS, NW), BF16), v((ROWS, NW), BF16), v((ROWS, NW), BF16),
        v((ROWS, NW), BF16), v((ROWS, NW), BF16), v((4, ROWS + 8, 128), F32),
        v((ROWS, NW), BF16), v((HALF, NW), BF16), v((ROWS, NW), BF16), v((HALF, NW), BF16),
        v((ROWS, NW), F32), v((BLOCKS, HEADS, 128, 128), F32),
        v((BLOCKS, HEADS, 128, 128), BF16), v((HALF, D), F32),
        v((ROWS, 128), F32), v((128, 128), F32), v((128, 128), F32),
        v((ROWS, 128), F32), v((ROWS, 128), F32),
        v((4, 128, 128), F32), v((16, 128), F32), v((1, D), BF16), v((HEADS, ROWS), F32),
        v((3, NW), BF16), v((128, 128), F32), v((128, 128), F32),
        v((BLOCKS, HEADS, 128, 128), F32), v((4, 8, 128), F32), v((4, 2, 8, 128), F32),
        v((4, 2, 128, 128), BF16), v((4, 2, 128, 128), BF16),
        v((4, 2, 128, 128), BF16), v((4, 2, 128, 128), BF16),
        v((3, 2, 128, 128), BF16), v((2, 128, 128), F32),
        dma((3,)), dma((5,)), dma((12,)), dma((4,)),
    ] + [dma((3,))] * 14 + [dma] * 8
    anywhere = pl.BlockSpec(memory_space=pl.ANY)
    return pl.pallas_call(
        kernel,
        out_shape=jax.ShapeDtypeStruct((HALF, D), BF16),
        in_specs=[anywhere] * 14,
        out_specs=pl.BlockSpec(memory_space=pltpu.VMEM),
        scratch_shapes=scratch,
        compiler_params=pltpu.CompilerParams(
            collective_id=0, has_side_effects=True, vmem_limit_bytes=62 * 1024 * 1024
        ),
    )(
        tokens, norm_gain.reshape(1, D), log_decay, conv_taps, w_key, w_value, w_query,
        w_conv_in, w_conv_pre, w_conv_post, w_out_conv, w_out_ret,
        jnp.asarray(within), jnp.asarray(bases),
    )


def solution(mesh):
    in_specs = (
        P(("fs", "sp"), "tp"),
        P(),
        P(None, "tp"),
        P(None, "tp"),
        P(None, "tp"),
        P("tp", "sp"),
        P(None, "tp"),
        P(None, "tp"),
        P(None, "tp"),
        P(None, "tp"),
        P(),
        P(),
    )
    out_specs = P(("fs", "sp", "tp"), None)
    return jax.shard_map(body, mesh=mesh, in_specs=in_specs, out_specs=out_specs, check_vma=False)
```

time: 132 us -> 43.5 us (0.33)
  Pallas kernels: 0 us -> 39.3 us
  matrix products: 31.5 us -> 0 us
  local copies, waits for them, and re-layouts: 31.4 us -> 4.02 us
  other arithmetic: 22.6 us -> 0 us
  starting transfers between devices: 18.9 us -> 0 us
  between operations: 13.9 us -> 0.01 us
  blocking collectives: 9.89 us -> 0 us
  waiting for transfers between devices: 2.86 us -> 0 us
    pallas_call x0 -> x1, Pallas kernels: none -> 39.3 us  [body(): pl.pallas_call(kernel, out_shape=jax.ShapeDtypeStruct((HALF, D), BF16), i...]
    dot_general x11 -> x0, matrix products: 31.5 us -> none  [the longest x6 17.7 us: project(): return jnp.dot(normed, weight, preferred_element_type=jnp.float32)]
    all_to_all x2 -> x0, starting transfers between devices: 15.1 us -> none  [copy_for_each(): lax.all_to_all(jnp.broadcast_to(shard[None], (devices, *shard.shape)), ax...]
    concatenate x8 -> x0, local copies, waits for them, and re-layouts: 11.7 us -> none  [rotate(): jnp.concatenate([leading * cosines - trailing * sinusoid, leading * sinus...]
    all_to_all x1 -> x0, blocking collectives: 9.89 us -> none  [summed_on_arrival(): lax.all_to_all(tiles, axis, split_axis=0, concat_axis=0, tiled=True)]
    reduce_sum x3 -> x0, other arithmetic: 7.11 us -> none  [the longest x1 4.21 us: summed_on_arrival(): return arrived.astype(jnp.float32).sum(axis=0)]
    exp x9 -> x0, local copies, waits for them, and re-layouts: 4.83 us -> none  [the longest x6 4.12 us: advance(): return (jnp.exp(end_decay)[:, None, None] * carried + fresh_state, carried)]
    dynamic_update_slice x6 -> x0, other arithmetic: 4.36 us -> none  [body(): lax.scan(advance, empty_state, (block_ends, block_states))]
  transfers between devices with their start and end apart: 4 -> 0, of which waited for: 1 -> 0; matrix products, arithmetic and copies ran while one was open for 32% -> 0% of each run, Pallas kernels for 0% -> 0%
where the time goes in v1:
time: 43.5 us; the launch traced here: 43.4 us
  Pallas kernels  39.3 us (90%)
  local copies, waits for them, and re-layouts  4.02 us (9%)
    pallas_call x1, Pallas kernels, body(): pl.pallas_call(kernel, out_shape=jax.ShapeDtypeStruct((HALF, D), BF16), i...  39.3 us
    unnamed x1, local copies, waits for them, and re-layouts  2.73 us
    reshape x1, local copies, waits for them, and re-layouts, body(): norm_gain.reshape(1, D)  1.29 us

profile of v1, /device:TPU:1, one launch (start us, length us, event | category | flops | bytes accessed | tf_op | source)
XLA Modules:
  0.0 43.4 jit_solution(14828161654727642127)
XLA Ops:
  0.0 1.3 %reshape.3.gain = bf16[1,2048]{1,0:T(2,128)(2,1)} reshape(bf16[2048]{0:T(1024)(128)(2,1)} %param.15) | data formatting | bytes 8192 | tf_op jit(solution)/shard_map/reshape | solution.py:564
  1.3 39.3 %shard_map.136 = bf16[384,2048]{1,0:T(8,128)(2,1)} custom-call(bf16[768,1024]{1,0:T(8,128)(2,1)} %tok.1, bf16[1,2048]{1,0:T(2,128)(2,1)} %reshape.3.gain, f32[4,768]{1,0:T(4,128)} %ld.1, bf16[3,512]{1,0:T(4,128)(2,1)} %taps.1, bf16[2048,512]{1,0:T(8,128)(2,1)} %wk.1, bf16[2048,512]{1,0:T(8,128)(2,1)} %wv.1, bf16[2048,512]{1,0:T(8,128)(2,1)} %wq.1, ...), custom_call_target="tpu_custom_call" | custom-call | tf_op jit(solution)/shard_map/pallas_call | solution.py:554
  40.6 2.7 %copy.16 = bf16[384,2048]{1,0:T(8,128)(2,1)} copy(bf16[384,2048]{1,0:T(8,128)(2,1)} %shard_map.136) | data formatting | bytes 3145728

commit v2 on v1

--- a/solution.py
+++ b/solution.py
@@ -51,9 +51,9 @@
     tok, gain, ld, taps, wk, wv, wq, wci, wcp, wcq, woc, wor, tabs, bases,
     out,
     xo, go, gp, wbuf, wob, acc, kb, vb, qb, cib, postb, gbuf, cob, cor,
-    retb, retr, inside, states, starts, oacc, ssb, pack, pack_far, rot_c, rot_s,
+    retb, retr, inside, starts, oacc, ssb, pack, pack_far, rot_c, rot_s,
     tabv, basev, gainv, ldv, tapv, ldp, cumr, colrep, lrow, lcol,
-    a1, a2, b1, b2, bm, pre,
+    a1, a2, b1, b2, bm, pre, fade, tails, cumc, endr, qs, entry, both,
     sem_tok, sem_small, sem_w, sem_wo,
     ts, tr, l1s, l1r, l2s, l2r, a1s, a1r, a2s, a2r, b1s, b1r, b2s, b2r,
     hs, hr, cs, cr, rs, rr, ps, pr,
@@ -125,6 +125,22 @@
     small[3].start()
     small[2].start()
 
+    lane = lax.broadcasted_iota(jnp.int32, (SPAN, SPAN), 1)
+    packed = jnp.zeros((SPAN, SPAN), F32)
+    for i in range(BLOCKS):
+        if i % 2 == 0:
+            tok_load[i // 2].wait()
+        rows = slice(i * 128, i * 128 + 128)
+        value = xo[rows, :].astype(F32)
+        squares = jnp.sum(value * value, axis=1, keepdims=True)
+        spread = jnp.broadcast_to(squares, (SPAN, SPAN))
+        ssb[rows, :] = spread
+        packed = jnp.where(lane == i, spread, packed)
+    pack[...] = packed
+
+    pl.semaphore_wait(barrier, 9)
+    pack_send = remote(pack, pack_far, ps, pr, {"tp": other})
+    pack_send.start()
     ldp[...] = jnp.zeros_like(ldp)
     small[0].wait()
     for b in range(BLOCKS):
@@ -141,38 +157,20 @@
         total = total + mm(piece, ones)
         rest = rest - piece.astype(F32)
     cumr[...] = total
-    columns = total.T
-    for b in range(BLOCKS):
-        for h in range(HEADS):
-            i = b * 8 + h
-            colrep[b, h] = jnp.broadcast_to(columns[:, i : i + 1], (SPAN, SPAN))
+    cumc[...] = total.T
+    ends = jnp.broadcast_to(total[:, SPAN - 1 : SPAN], (SPAN, SPAN))
+    endr[...] = ends
+    whole = ends[0:8]
+    for b in range(1, BLOCKS):
+        whole = whole + ends[b * 8 : b * 8 + 8]
+    lrow[x] = whole
 
     def block_end(b, h):
-        return colrep[b, h, SPAN - 1 : SPAN, :]
-
-    lrow[x] = jnp.zeros((8, SPAN), F32)
-    for h in range(HEADS):
-        whole = block_end(0, h)
-        for b in range(1, BLOCKS):
-            whole = whole + block_end(b, h)
-        lrow[x, h : h + 1, :] = whole
-
-    lane = lax.broadcasted_iota(jnp.int32, (SPAN, SPAN), 1)
-    packed = jnp.zeros((SPAN, SPAN), F32)
-    for i in range(BLOCKS):
-        if i % 2 == 0:
-            tok_load[i // 2].wait()
-        rows = slice(i * 128, i * 128 + 128)
-        value = xo[rows, :].astype(F32)
-        squares = jnp.sum(value * value, axis=1, keepdims=True)
-        spread = jnp.broadcast_to(squares, (SPAN, SPAN))
-        ssb[rows, :] = spread
-        packed = jnp.where(lane == i, spread, packed)
-    pack[...] = packed
-
-    pl.semaphore_wait(barrier, 9)
-    pack_send = remote(pack, pack_far, ps, pr, {"tp": other})
-    pack_send.start()
+        return endr[b * 8 + h : b * 8 + h + 1, :]
+
+    def section(body):
+        pl.when(sp < 16)(body)
+
     l1_send = [
         remote(lrow.at[x], lrow.at[x], l1s.at[k], l1r.at[k], {"sp": row_peer[k]})
         for k in range(3)
@@ -180,22 +178,9 @@
     for copy in l1_send:
         copy.start()
     w_load("wq", 0).start()
-    w_load("wci", 0).start()
 
     small[1].wait()
-    small[3].wait()
-    small[4].wait()
-
-    def tables(b, carry):
-        rows = pl.ds(pl.multiple_of(b * 128, 128), 128)
-        base_c = basev[pl.ds(b, 1), :]
-        base_s = basev[pl.ds(b + 8, 1), :]
-        rot_c[rows, :] = base_c * tabv[0] - base_s * tabv[1]
-        rot_s[rows, :] = base_s * tabv[2] + base_c * tabv[3]
-        return carry
-
-    lax.fori_loop(0, BLOCKS, tables, 0)
-    weight = gainv[:, pl.ds(own_k, KW)].astype(F32)
+    weight = gainv[pl.ds(own_k, KW)].astype(F32).reshape(1, KW)
     pack_send.wait_recv()
     tok_send = [
         remote(
@@ -215,29 +200,45 @@
             tok_send[i // 2 - 1].start()
     tok_send[2].start()
 
-    def near_product(name):
-        i = index[name]
+    lower = (
+        lax.broadcasted_iota(jnp.int32, (SPAN, SPAN), 0)
+        >= lax.broadcasted_iota(jnp.int32, (SPAN, SPAN), 1)
+    )
+
+    def near_product(i):
+        for n in range(2):
+            cols = slice(n * 256, n * 256 + 256)
+            acc[i, :, cols] = mm(go[...], wbuf[i, 0, :, cols])
+
+    for name in ("wk", "wv", "wq"):
         w_load(name, 0).wait()
-
-        def step(n, carry):
-            cols = pl.ds(pl.multiple_of(n * 256, 256), 256)
-            acc[i, :, cols] = mm(go[...], wbuf[i, 0, :, cols])
-            return carry
-
-        lax.fori_loop(0, 2, step, 0)
-
-    near_product("wk")
-    w_load("wk", 1).start()
-    w_load("wv", 1).start()
-    near_product("wv")
-    w_load("wq", 1).start()
-    w_load("wci", 1).start()
-    near_product("wq")
-    w_load("wcp", 0).start()
-    w_load("wcp", 1).start()
-    near_product("wci")
-    w_load("wcq", 0).start()
-    w_load("wcq", 1).start()
+    for name in ("wk", "wv", "wq"):
+        w_load(name, 1).start()
+    for name in ("wci", "wcp"):
+        for part in range(2):
+            w_load(name, part).start()
+    small[3].wait()
+    small[4].wait()
+
+    @section
+    def _():
+        near_product(0)
+        for b in range(BLOCKS):
+            rows = slice(b * 128, b * 128 + 128)
+            base_c = basev[b : b + 1, :]
+            base_s = basev[b + 8 : b + 9, :]
+            rot_c[rows, :] = base_c * tabv[0] - base_s * tabv[1]
+            rot_s[rows, :] = base_s * tabv[2] + base_c * tabv[3]
+        near_product(1)
+        for b in range(BLOCKS):
+            for h in range(HEADS):
+                i = b * 8 + h
+                column = jnp.broadcast_to(cumc[:, i : i + 1], (SPAN, SPAN))
+                colrep[b, h] = column
+                gap = column - cumr[i : i + 1, :]
+                fade[b, h] = jnp.where(lower, jnp.exp(jnp.minimum(gap, 0.0)), 0.0)
+                tails[b, h] = jnp.exp(block_end(b, h) - column)
+        near_product(2)
 
     for copy in l1_send:
         copy.wait_recv()
@@ -266,20 +267,17 @@
         return value * rot_c[...] + pltpu.roll(value, 64, axis=1) * rot_s[...]
 
     exchange = []
-    for n in range(2):
+
+    def key_value(n):
         cols = slice(n * 256, n * 256 + 256)
-        if n == 0:
-            w_load("wk", 1).wait()
         kk = acc[0, :, cols] + mm(gp[...], wbuf[0, 1, :, cols])
         for j in range(2):
             at = slice(n * 256 + j * 128, n * 256 + j * 128 + 128)
             kb[:, at] = (rotated(kk[:, j * 128 : j * 128 + 128]) * KEY_SCALE).astype(BF16)
-        if n == 0:
-            w_load("wv", 1).wait()
         vv = acc[1, :, cols] + mm(gp[...], wbuf[1, 1, :, cols])
-        for j in range(2):
-            at = slice(n * 256 + j * 128, n * 256 + j * 128 + 128)
-            vb[:, at] = vv[:, j * 128 : j * 128 + 128].astype(BF16)
+        vb[:, cols] = vv.astype(BF16)
+
+    def fresh_states(n):
         slot = a1.at[x] if n == 0 else b1.at[z]
         for j in range(2):
             h = n * 2 + j
@@ -287,16 +285,19 @@
             whole = None
             for b in range(BLOCKS):
                 rows = slice(b * 128, b * 128 + 128)
-                end = block_end(b, h)
-                tail = jnp.exp(end - colrep[b, h])
-                weighted = (vb[rows, at].astype(F32) * tail).astype(BF16)
+                weighted = (vb[rows, at].astype(F32) * tails[b, h]).astype(BF16)
                 fresh = lax.dot_general(
                     kb[rows, at], weighted, (((0,), (0,)), ((), ())),
                     preferred_element_type=F32,
                 )
-                states[b, h] = fresh
-                whole = fresh if whole is None else jnp.exp(end) * whole + fresh
+                if b == 0:
+                    whole = fresh
+                else:
+                    starts[b, h] = whole.astype(BF16)
+                    whole = jnp.exp(block_end(b, h)) * whole + fresh
             slot[j] = whole.astype(BF16)
+
+    def send_states(n):
         for k in range(3):
             if n == 0:
                 copy = remote(a1.at[x], a1.at[x], a1s.at[k], a1r.at[k], {"sp": row_peer[k]})
@@ -305,48 +306,59 @@
             copy.start()
             exchange.append(copy)
 
-    w_load("wq", 1).wait()
-
-    def query_step(n, carry):
-        cols = pl.ds(pl.multiple_of(n * 256, 256), 256)
-        qq = acc[2, :, cols] + mm(gp[...], wbuf[2, 1, :, cols])
-        for j in range(2):
-            at = pl.ds(pl.multiple_of(n * 256 + j * 128, 128), 128)
-            qb[:, at] = rotated(qq[:, j * 128 : j * 128 + 128]).astype(BF16)
-        return carry
-
-    lax.fori_loop(0, 2, query_step, 0)
-
-    w_load("wci", 1).wait()
-
-    def conv_in_step(n, carry):
-        cols = pl.ds(pl.multiple_of(n * 256, 256), 256)
-        value = acc[3, :, cols] + mm(gp[...], wbuf[3, 1, :, cols])
-        cib[:, cols] = value.astype(BF16)
-        return carry
-
-    lax.fori_loop(0, 2, conv_in_step, 0)
-
-    w_load("wcp", 0).wait()
-    w_load("wcp", 1).wait()
+    for name in ("wk", "wv", "wq"):
+        w_load(name, 1).wait()
+    @section
+    def _():
+        key_value(0)
+        key_value(1)
+
+    @section
+    def _():
+        fresh_states(0)
+        fresh_states(1)
+
+    send_states(0)
+    send_states(1)
+
+    for name in ("wci", "wcp"):
+        for part in range(2):
+            w_load(name, part).wait()
+    for part in range(2):
+        w_load("wcq", part).start()
     for i in range(2):
         for part in range(2):
             wo_load(i, part).start()
 
-    def conv_pre_step(n, carry):
-        cols = pl.ds(pl.multiple_of(n * 256, 256), 256)
-        value = mm(go[...], wbuf[4, 0, :, cols]) + mm(gp[...], wbuf[4, 1, :, cols])
-        pre_gate = value.astype(BF16).astype(F32)
-        gated = (pre_gate * cib[:, cols].astype(F32)).astype(BF16).astype(F32)
-        for j in range(2):
-            gbuf[n * 2 + j, 8 : 8 + ROWS, :] = gated[:, j * 128 : j * 128 + 128]
-        return carry
-
-    lax.fori_loop(0, 2, conv_pre_step, 0)
+    def full_product(i, cols):
+        return (
+            mm(go[...], wbuf[i, 0, :, cols]) + mm(gp[...], wbuf[i, 1, :, cols])
+        ).astype(BF16)
+
+    @section
+    def _():
+        for n in range(2):
+            cols = slice(n * 256, n * 256 + 256)
+            cib[:, cols] = full_product(3, cols)
+            gated = full_product(4, cols).astype(F32) * cib[:, cols].astype(F32)
+            gated = gated.astype(BF16).astype(F32)
+            for j in range(2):
+                gbuf[n * 2 + j, 8 : 8 + ROWS, :] = gated[:, j * 128 : j * 128 + 128]
+
     halo = remote(
         gbuf.at[:, pl.ds(ROWS, 8), :], gbuf.at[:, pl.ds(0, 8), :], hs, hr, {"sp": after}
     )
     halo.start()
+
+    @section
+    def _():
+        for n in range(2):
+            cols = slice(n * 256, n * 256 + 256)
+            qq = acc[2, :, cols] + mm(gp[...], wbuf[2, 1, :, cols])
+            for j in range(2):
+                at = slice(n * 256 + j * 128, n * 256 + j * 128 + 128)
+                qb[:, at] = rotated(qq[:, j * 128 : j * 128 + 128]).astype(BF16)
+
 
     for copy in l2_send:
         copy.wait_recv()
@@ -404,16 +416,13 @@
         copy.start()
         second.append(copy)
 
-    w_load("wcq", 0).wait()
-    w_load("wcq", 1).wait()
-
-    def conv_post_step(n, carry):
-        cols = pl.ds(pl.multiple_of(n * 256, 256), 256)
-        value = mm(go[...], wbuf[5, 0, :, cols]) + mm(gp[...], wbuf[5, 1, :, cols])
-        postb[:, cols] = value.astype(BF16)
-        return carry
-
-    lax.fori_loop(0, 2, conv_post_step, 0)
+    for part in range(2):
+        w_load("wcq", part).wait()
+    @section
+    def _():
+        for n in range(2):
+            cols = slice(n * 256, n * 256 + 256)
+            postb[:, cols] = full_product(5, cols)
 
     small[2].wait()
     halo.wait_recv()
@@ -422,49 +431,62 @@
     def _():
         gbuf[:, 0:8, :] = jnp.zeros((4, 8, 128), F32)
 
-    for c in range(4):
-        at = slice(c * 128, c * 128 + 128)
-        summed = jnp.zeros((ROWS, 128), F32)
-        for i in range(3):
-            summed = summed + tapv[i : i + 1, at].astype(F32) * gbuf[c, 6 + i : 6 + i + ROWS, :]
-        cob[:, at] = (postb[:, at].astype(F32) * summed).astype(BF16)
+    @section
+    def _():
+        for c in range(4):
+            at = slice(c * 128, c * 128 + 128)
+            summed = jnp.zeros((ROWS, 128), F32)
+            for i in range(3):
+                summed = summed + tapv[i : i + 1, at].astype(F32) * gbuf[c, 6 + i : 6 + i + ROWS, :]
+            cob[:, at] = (postb[:, at].astype(F32) * summed).astype(BF16)
+
     conv_send = remote(cob.at[far_rows, :], cor, cs, cr, {"tp": other})
     conv_send.start()
 
-    lower = (
-        lax.broadcasted_iota(jnp.int32, (SPAN, SPAN), 0)
-        >= lax.broadcasted_iota(jnp.int32, (SPAN, SPAN), 1)
-    )
-
-    def inside_step(b, carry):
-        rows = pl.ds(pl.multiple_of(b * 128, 128), 128)
-        for h in range(HEADS):
-            at = slice(h * 128, h * 128 + 128)
-            gap = colrep[b, h] - cumr[pl.ds(b * 8 + h, 1), :]
-            weight = jnp.where(lower, jnp.exp(jnp.minimum(gap, 0.0)), 0.0)
-            scores = lax.dot_general(
-                qb[rows, at], kb[rows, at], (((1,), (1,)), ((), ())),
-                preferred_element_type=F32,
-            )
-            mixed = (scores * weight).astype(BF16)
-            inside[rows, at] = mm(mixed, vb[rows, at])
-        return carry
-
-    lax.fori_loop(0, BLOCKS, inside_step, 0)
-
-    conv_send.wait_recv()
+    @section
+    def _():
+        for b in range(BLOCKS):
+            rows = slice(b * 128, b * 128 + 128)
+            for h in range(HEADS):
+                at = slice(h * 128, h * 128 + 128)
+                scores = lax.dot_general(
+                    qb[rows, at], kb[rows, at], (((1,), (1,)), ((), ())),
+                    preferred_element_type=F32,
+                )
+                both[b, h, :, :128] = (scores * fade[b, h]).astype(BF16)
+                query = qb[rows, at].astype(F32)
+                if b == 0:
+                    qs[rows, at] = (query * jnp.exp(colrep[b, h])).astype(BF16)
+                else:
+                    both[b, h, :, 128:] = (query * jnp.exp(colrep[b, h])).astype(BF16)
+                    offset = endr[h : h + 1, :]
+                    for e in range(1, b):
+                        offset = offset + block_end(e, h)
+                    qs[rows, at] = (query * jnp.exp(colrep[b, h] + offset)).astype(BF16)
+        for b in range(BLOCKS):
+            rows = slice(b * 128, b * 128 + 128)
+            for h in range(HEADS):
+                at = slice(h * 128, h * 128 + 128)
+                if b == 0:
+                    inside[rows, at] = mm(both[b, h, :, :128], vb[rows, at])
+                else:
+                    inside[rows, at] = mm(
+                        both[b, h],
+                        jnp.concatenate([vb[rows, at], starts[b, h]], axis=0),
+                    )
+
     for i in range(2):
         for part in range(2):
             wo_load(i, part).wait()
-
-    def out_conv_step(n, carry):
-        cols = pl.ds(pl.multiple_of(n * 512, 512), 512)
-        oacc[:, cols] = mm(cob[own_rows, :], wob[0, 0, :, cols]) + mm(
-            cor[...], wob[0, 1, :, cols]
-        )
-        return carry
-
-    lax.fori_loop(0, 4, out_conv_step, 0)
+    conv_send.wait_recv()
+
+    @section
+    def _():
+        for n in range(8):
+            cols = slice(n * 256, n * 256 + 256)
+            oacc[:, cols] = mm(cob[own_rows, :], wob[0, 0, :, cols]) + mm(
+                cor[...], wob[0, 1, :, cols]
+            )
 
     for k in range(6):
         second[k].wait_recv()
@@ -481,45 +503,35 @@
             state = b2[0, j].astype(F32)
             for i in range(1, 4):
                 state = state + b2[i, j].astype(F32)
-        for b in range(BLOCKS):
-            starts[b, h] = state.astype(BF16)
-            if b < BLOCKS - 1:
-                state = jnp.exp(block_end(b, h)) * state + states[b, h]
+        entry[h] = state.astype(BF16)
 
     def across(first):
-        def step(i, carry):
-            b = first + i
-            rows = pl.ds(pl.multiple_of(b * 128, 128), 128)
+        for i in range(3):
+            rows = pl.ds(pl.multiple_of(first + i * 128, 128), 128)
             for h in range(HEADS):
                 at = slice(h * 128, h * 128 + 128)
-                value = inside[rows, at] + jnp.exp(colrep[b, h]) * mm(
-                    qb[rows, at], starts[b, h]
-                )
+                value = inside[rows, at] + mm(qs[rows, at], entry[h])
                 level = jnp.mean(value * value, axis=1, keepdims=True)
                 retb[rows, at] = (value * lax.rsqrt(level + EPS)).astype(BF16)
-            return carry
-
-        lax.fori_loop(0, 3, step, 0)
-
-    across(other * 3)
+
+    section(lambda: across(other * HALF))
     ret_send = remote(retb.at[far_rows, :], retr, rs, rr, {"tp": other})
     ret_send.start()
-    across(tp * 3)
-
-    def out_near_step(n, carry):
-        cols = pl.ds(pl.multiple_of(n * 512, 512), 512)
-        oacc[:, cols] += mm(retb[own_rows, :], wob[1, 0, :, cols])
-        return carry
-
-    lax.fori_loop(0, 4, out_near_step, 0)
+    section(lambda: across(tp * HALF))
+
+    @section
+    def _():
+        for n in range(8):
+            cols = slice(n * 256, n * 256 + 256)
+            oacc[:, cols] += mm(retb[own_rows, :], wob[1, 0, :, cols])
+
     ret_send.wait_recv()
 
-    def out_far_step(n, carry):
-        cols = pl.ds(pl.multiple_of(n * 512, 512), 512)
-        out[:, cols] = (oacc[:, cols] + mm(retr[...], wob[1, 1, :, cols])).astype(BF16)
-        return carry
-
-    lax.fori_loop(0, 4, out_far_step, 0)
+    @section
+    def _():
+        for n in range(8):
+            cols = slice(n * 256, n * 256 + 256)
+            out[:, cols] = (oacc[:, cols] + mm(retr[...], wob[1, 1, :, cols])).astype(BF16)
 
     for copy in [pack_send] + tok_send + l1_send + l2_send + exchange + second + [halo, conv_send, ret_send]:
         copy.wait_send()
@@ -534,34 +546,37 @@
     v = pltpu.VMEM
     scratch = [
         v((ROWS, KW), BF16), v((ROWS, KW), BF16), v((ROWS, KW), BF16),
-        v((6, 2, KW, NW), BF16), v((2, 2, NW, D), BF16), v((4, ROWS, NW), F32),
+        v((6, 2, KW, NW), BF16), v((2, 2, NW, D), BF16), v((3, ROWS, NW), F32),
         v((ROWS, NW), BF16), v((ROWS, NW), BF16), v((ROWS, NW), BF16),
         v((ROWS, NW), BF16), v((ROWS, NW), BF16), v((4, ROWS + 8, 128), F32),
         v((ROWS, NW), BF16), v((HALF, NW), BF16), v((ROWS, NW), BF16), v((HALF, NW), BF16),
-        v((ROWS, NW), F32), v((BLOCKS, HEADS, 128, 128), F32),
+        v((ROWS, NW), F32),
         v((BLOCKS, HEADS, 128, 128), BF16), v((HALF, D), F32),
         v((ROWS, 128), F32), v((128, 128), F32), v((128, 128), F32),
         v((ROWS, 128), F32), v((ROWS, 128), F32),
-        v((4, 128, 128), F32), v((16, 128), F32), v((1, D), BF16), v((HEADS, ROWS), F32),
+        v((4, 128, 128), F32), v((16, 128), F32), v((D,), BF16), v((HEADS, ROWS), F32),
         v((3, NW), BF16), v((128, 128), F32), v((128, 128), F32),
         v((BLOCKS, HEADS, 128, 128), F32), v((4, 8, 128), F32), v((4, 2, 8, 128), F32),
         v((4, 2, 128, 128), BF16), v((4, 2, 128, 128), BF16),
         v((4, 2, 128, 128), BF16), v((4, 2, 128, 128), BF16),
         v((3, 2, 128, 128), BF16), v((2, 128, 128), F32),
+        v((BLOCKS, HEADS, 128, 128), F32), v((BLOCKS, HEADS, 128, 128), F32),
+        v((128, 128), F32), v((128, 128), F32), v((ROWS, NW), BF16), v((HEADS, 128, 128), BF16),
+        v((BLOCKS, HEADS, 128, 256), BF16),
         dma((3,)), dma((5,)), dma((12,)), dma((4,)),
     ] + [dma((3,))] * 14 + [dma] * 8
-    anywhere = pl.BlockSpec(memory_space=pl.ANY)
+    anywhere = pl.BlockSpec(memory_space=pltpu.HBM)
     return pl.pallas_call(
         kernel,
-        out_shape=jax.ShapeDtypeStruct((HALF, D), BF16),
+        out_shape=pltpu.VMEM((HALF, D), BF16),
         in_specs=[anywhere] * 14,
         out_specs=pl.BlockSpec(memory_space=pltpu.VMEM),
         scratch_shapes=scratch,
         compiler_params=pltpu.CompilerParams(
-            collective_id=0, has_side_effects=True, vmem_limit_bytes=62 * 1024 * 1024
+            collective_id=0, has_side_effects=True, vmem_limit_bytes=56 * 1024 * 1024
         ),
     )(
-        tokens, norm_gain.reshape(1, D), log_decay, conv_taps, w_key, w_value, w_query,
+        tokens, norm_gain, log_decay, conv_taps, w_key, w_value, w_query,
         w_conv_in, w_conv_pre, w_conv_post, w_out_conv, w_out_ret,
         jnp.asarray(within), jnp.asarray(bases),
     )

time: 43.5 us -> 30 us (0.69)
  Pallas kernels: 39.3 us -> 28.7 us
  local copies, waits for them, and re-layouts: 4.02 us -> 1.15 us
    pallas_call x1, Pallas kernels: 39.3 us -> 28.7 us  [body(): pl.pallas_call(kernel, out_shape=pltpu.VMEM((HALF, D), BF16), in_specs=[a...]
    unnamed x1, local copies, waits for them, and re-layouts: 2.73 us -> 1.15 us
    reshape x1 -> x0, local copies, waits for them, and re-layouts: 1.29 us -> none  [body(): norm_gain.reshape(1, D)]
where the time goes in v2:
time: 30 us; the launch traced here: 29.8 us
  Pallas kernels  28.7 us (96%)
  local copies, waits for them, and re-layouts  1.15 us (4%)
    pallas_call x1, Pallas kernels, body(): pl.pallas_call(kernel, out_shape=pltpu.VMEM((HALF, D), BF16), in_specs=[a...  28.7 us
    unnamed x1, local copies, waits for them, and re-layouts  1.15 us

profile of v2, /device:TPU:1, one launch (start us, length us, event | category | flops | bytes accessed | tf_op | source)
XLA Modules:
  0.0 29.8 jit_solution(4287723980700130366)
XLA Ops:
  0.0 28.7 %shard_map.136 = bf16[384,2048]{1,0:T(8,128)(2,1)S(1)} custom-call(bf16[768,1024]{1,0:T(8,128)(2,1)} %tok.1, bf16[2048]{0:T(1024)(128)(2,1)} %gain.1, f32[4,768]{1,0:T(4,128)} %ld.1, bf16[3,512]{1,0:T(4,128)(2,1)} %taps.1, bf16[2048,512]{1,0:T(8,128)(2,1)} %wk.1, bf16[2048,512]{1,0:T(8,128)(2,1)} %wv.1, bf16[2048,512]{1,0:T(8,128)(2,1)} %wq.1, ...), custom_call_target="tpu_custom_call" | custom-call | tf_op jit(solution)/shard_map/pallas_call | solution.py:569
  28.7 1.1 %copy.16 = bf16[384,2048]{1,0:T(8,128)(2,1)} copy(bf16[384,2048]{1,0:T(8,128)(2,1)S(1)} %shard_map.136) | data formatting | bytes 3145728

commit v3 on v2

--- a/solution.py
+++ b/solution.py
@@ -52,11 +52,11 @@
     out,
     xo, go, gp, wbuf, wob, acc, kb, vb, qb, cib, postb, gbuf, cob, cor,
     retb, retr, inside, starts, oacc, ssb, pack, pack_far, rot_c, rot_s,
-    tabv, basev, gainv, ldv, tapv, ldp, cumr, colrep, lrow, lcol,
+    tabv, basev, gainv, ldv, tapv, ldp, cumr, colrep, lall,
     a1, a2, b1, b2, bm, pre, fade, tails, cumc, endr, qs, entry, both,
     sem_tok, sem_small, sem_w, sem_wo,
-    ts, tr, l1s, l1r, l2s, l2r, a1s, a1r, a2s, a2r, b1s, b1r, b2s, b2r,
-    hs, hr, cs, cr, rs, rr, ps, pr,
+    ts, tr, ls, lr, a1s, a1r, a2s, a2r, b1s, b1r, b2s, b2r,
+    hs, hr, cs, cr, rs, rr, ps, pr, met,
 ):
     sp = lax.axis_index("sp")
     tp = lax.axis_index("tp")
@@ -66,12 +66,17 @@
     row_peer = [z * 4 + lax.rem(x + k, 4) for k in (1, 2, 3)]
     col_peer = [lax.rem(z + k, 4) * 4 + x for k in (1, 2, 3)]
     after = lax.rem(sp + 1, 16)
-    before = lax.rem(sp + 15, 16)
+    ahead = [lax.rem(sp + k, 16) for k in range(1, 16)]
+    behind = [lax.rem(sp + 16 - k, 16) for k in range(1, 16)]
 
     barrier = pltpu.get_barrier_semaphore()
-    pl.semaphore_signal(barrier, inc=1, device_id={"tp": other}, device_id_type=MESH)
-    for peer in row_peer + col_peer + [after, before]:
-        pl.semaphore_signal(barrier, inc=1, device_id={"sp": peer}, device_id_type=MESH)
+    lall[...] = jnp.zeros_like(lall)
+    a2[...] = jnp.zeros_like(a2)
+    b1[...] = jnp.zeros_like(b1)
+
+    @pl.when(tp == 0)
+    def _():
+        pl.semaphore_signal(barrier, inc=1, device_id={"tp": 1}, device_id_type=MESH)
 
     def remote(src, dst, send, recv, where):
         return pltpu.make_async_remote_copy(
@@ -138,7 +143,17 @@
         packed = jnp.where(lane == i, spread, packed)
     pack[...] = packed
 
-    pl.semaphore_wait(barrier, 9)
+    @pl.when(tp == 1)
+    def _():
+        pl.semaphore_wait(barrier, 1)
+        pl.semaphore_signal(met, inc=1, device_id={"tp": 0}, device_id_type=MESH)
+
+    @pl.when(tp == 0)
+    def _():
+        pl.semaphore_wait(met, 1)
+        for peer in ahead:
+            pl.semaphore_signal(barrier, inc=1, device_id={"sp": peer}, device_id_type=MESH)
+
     pack_send = remote(pack, pack_far, ps, pr, {"tp": other})
     pack_send.start()
     ldp[...] = jnp.zeros_like(ldp)
@@ -163,7 +178,7 @@
     whole = ends[0:8]
     for b in range(1, BLOCKS):
         whole = whole + ends[b * 8 : b * 8 + 8]
-    lrow[x] = whole
+    lall[sp] = whole
 
     def block_end(b, h):
         return endr[b * 8 + h : b * 8 + h + 1, :]
@@ -171,12 +186,6 @@
     def section(body):
         pl.when(sp < 16)(body)
 
-    l1_send = [
-        remote(lrow.at[x], lrow.at[x], l1s.at[k], l1r.at[k], {"sp": row_peer[k]})
-        for k in range(3)
-    ]
-    for copy in l1_send:
-        copy.start()
     w_load("wq", 0).start()
 
     small[1].wait()
@@ -240,26 +249,6 @@
                 tails[b, h] = jnp.exp(block_end(b, h) - column)
         near_product(2)
 
-    for copy in l1_send:
-        copy.wait_recv()
-    line = [lrow[i] for i in range(4)]
-
-    def between(low, high):
-        parts = [
-            jnp.where(jnp.logical_and(i > low, i < high), line[i], 0.0) for i in range(4)
-        ]
-        return (parts[0] + parts[1]) + (parts[2] + parts[3])
-
-    row_total = (line[0] + line[1]) + (line[2] + line[3])
-    lcol[z, 0] = row_total
-    lcol[z, 1] = between(x, 4)
-    l2_send = [
-        remote(lcol.at[z], lcol.at[z], l2s.at[k], l2r.at[k], {"sp": col_peer[k]})
-        for k in range(3)
-    ]
-    for copy in l2_send:
-        copy.start()
-
     for copy in tok_send:
         copy.wait_recv()
 
@@ -303,7 +292,7 @@
                 copy = remote(a1.at[x], a1.at[x], a1s.at[k], a1r.at[k], {"sp": row_peer[k]})
             else:
                 copy = remote(b1.at[z], b1.at[z], b1s.at[k], b1r.at[k], {"sp": col_peer[k]})
-            copy.start()
+            pl.when(True if n == 0 else z + k < 3)(copy.start)
             exchange.append(copy)
 
     for name in ("wk", "wv", "wq"):
@@ -312,6 +301,21 @@
     def _():
         key_value(0)
         key_value(1)
+
+    @pl.when(tp == 0)
+    def _():
+        pl.semaphore_wait(barrier, 15)
+        pl.semaphore_signal(met, inc=1, device_id={"tp": 1}, device_id_type=MESH)
+
+    @pl.when(tp == 1)
+    def _():
+        pl.semaphore_wait(met, 1)
+
+    def total_copy(k):
+        return remote(lall.at[sp], lall.at[sp], ls.at[k], lr.at[k], {"sp": ahead[k]})
+
+    for k in range(15):
+        pl.when(lax.div(ahead[k], 4) >= z)(total_copy(k).start)
 
     @section
     def _():
@@ -348,7 +352,7 @@
     halo = remote(
         gbuf.at[:, pl.ds(ROWS, 8), :], gbuf.at[:, pl.ds(0, 8), :], hs, hr, {"sp": after}
     )
-    halo.start()
+    pl.when(sp < 15)(halo.start)
 
     @section
     def _():
@@ -360,10 +364,22 @@
                 qb[:, at] = rotated(qq[:, j * 128 : j * 128 + 128]).astype(BF16)
 
 
-    for copy in l2_send:
-        copy.wait_recv()
-    row_sums = [lcol[i, 0] for i in range(4)]
-    suffix = [lcol[i, 1] for i in range(4)]
+    for k in range(15):
+        pl.when(lax.div(behind[k], 4) <= z)(total_copy(k).wait_recv)
+    totals = [[lall[4 * i + j] for j in range(4)] for i in range(4)]
+    line = [lall[4 * z + j] for j in range(4)]
+
+    def between(low, high):
+        parts = [
+            jnp.where(jnp.logical_and(i > low, i < high), line[i], 0.0) for i in range(4)
+        ]
+        return (parts[0] + parts[1]) + (parts[2] + parts[3])
+
+    row_sums = [(t[0] + t[1]) + (t[2] + t[3]) for t in totals]
+    suffix = []
+    for t in totals:
+        parts = [jnp.where(j > x, t[j], 0.0) for j in range(4)]
+        suffix.append((parts[0] + parts[1]) + (parts[2] + parts[3]))
     before_me = between(-1, x)
 
     def rows_between(low):
@@ -375,29 +391,12 @@
     def lane_row(weight, h):
         return weight[h : h + 1, :]
 
-    to_end = [jnp.exp(between(i, 4)) for i in range(4)]
-    to_me = [jnp.where(i < x, jnp.exp(between(i, x)), 0.0) for i in range(4)]
-    for k in range(3):
-        exchange[k].wait_recv()
-    for j in range(2):
-        parts = [a1[i, j].astype(F32) for i in range(4)]
-        row_state = lane_row(to_end[0], j) * parts[0]
-        prefix = lane_row(to_me[0], j) * parts[0]
-        for i in range(1, 4):
-            row_state = row_state + lane_row(to_end[i], j) * parts[i]
-            prefix = prefix + lane_row(to_me[i], j) * parts[i]
-        pre[j] = prefix
-        a2[z, j] = row_state.astype(BF16)
     second = []
-    for k in range(3):
-        copy = remote(a2.at[z], a2.at[z], a2s.at[k], a2r.at[k], {"sp": col_peer[k]})
-        copy.start()
-        second.append(copy)
     above = [
         jnp.where(i < z, jnp.exp(suffix[i] + rows_between(i)), 0.0) for i in range(4)
     ]
     for k in range(3):
-        exchange[3 + k].wait_recv()
+        pl.when(z > k)(exchange[3 + k].wait_recv)
     e_own = jnp.exp(before_me)
     for j in range(2):
         h = 2 + j
@@ -424,8 +423,26 @@
             cols = slice(n * 256, n * 256 + 256)
             postb[:, cols] = full_product(5, cols)
 
+    to_end = [jnp.exp(between(i, 4)) for i in range(4)]
+    to_me = [jnp.where(i < x, jnp.exp(between(i, x)), 0.0) for i in range(4)]
+    for k in range(3):
+        exchange[k].wait_recv()
+    for j in range(2):
+        parts = [a1[i, j].astype(F32) for i in range(4)]
+        row_state = lane_row(to_end[0], j) * parts[0]
+        prefix = lane_row(to_me[0], j) * parts[0]
+        for i in range(1, 4):
+            row_state = row_state + lane_row(to_end[i], j) * parts[i]
+            prefix = prefix + lane_row(to_me[i], j) * parts[i]
+        pre[j] = prefix
+        a2[z, j] = row_state.astype(BF16)
+    for k in range(3):
+        copy = remote(a2.at[z], a2.at[z], a2s.at[k], a2r.at[k], {"sp": col_peer[k]})
+        pl.when(z + k < 3)(copy.start)
+        second.append(copy)
+
     small[2].wait()
-    halo.wait_recv()
+    pl.when(sp > 0)(halo.wait_recv)
 
     @pl.when(sp == 0)
     def _():
@@ -488,8 +505,9 @@
                 cor[...], wob[0, 1, :, cols]
             )
 
-    for k in range(6):
+    for k in range(3):
         second[k].wait_recv()
+        pl.when(z > k)(second[3 + k].wait_recv)
     down = [
         jnp.where(i < z, jnp.exp(rows_between(i) + before_me), 0.0) for i in range(4)
     ]
@@ -533,8 +551,14 @@
             cols = slice(n * 256, n * 256 + 256)
             out[:, cols] = (oacc[:, cols] + mm(retr[...], wob[1, 1, :, cols])).astype(BF16)
 
-    for copy in [pack_send] + tok_send + l1_send + l2_send + exchange + second + [halo, conv_send, ret_send]:
+    for copy in [pack_send, conv_send, ret_send] + tok_send + exchange[:3] + second[:3]:
         copy.wait_send()
+    pl.when(sp < 15)(halo.wait_send)
+    for k in range(3):
+        pl.when(z + k < 3)(exchange[3 + k].wait_send)
+        pl.when(z + k < 3)(second[3 + k].wait_send)
+    for k in range(15):
+        pl.when(lax.div(ahead[k], 4) >= z)(total_copy(k).wait_send)
 
 
 def body(
@@ -556,7 +580,7 @@
         v((ROWS, 128), F32), v((ROWS, 128), F32),
         v((4, 128, 128), F32), v((16, 128), F32), v((D,), BF16), v((HEADS, ROWS), F32),
         v((3, NW), BF16), v((128, 128), F32), v((128, 128), F32),
-        v((BLOCKS, HEADS, 128, 128), F32), v((4, 8, 128), F32), v((4, 2, 8, 128), F32),
+        v((BLOCKS, HEADS, 128, 128), F32), v((16, 8, 128), F32),
         v((4, 2, 128, 128), BF16), v((4, 2, 128, 128), BF16),
         v((4, 2, 128, 128), BF16), v((4, 2, 128, 128), BF16),
         v((3, 2, 128, 128), BF16), v((2, 128, 128), F32),
@@ -564,7 +588,7 @@
         v((128, 128), F32), v((128, 128), F32), v((ROWS, NW), BF16), v((HEADS, 128, 128), BF16),
         v((BLOCKS, HEADS, 128, 256), BF16),
         dma((3,)), dma((5,)), dma((12,)), dma((4,)),
-    ] + [dma((3,))] * 14 + [dma] * 8
+    ] + [dma((3,))] * 2 + [dma((15,))] * 2 + [dma((3,))] * 8 + [dma] * 8 + [pltpu.SemaphoreType.REGULAR]
     anywhere = pl.BlockSpec(memory_space=pltpu.HBM)
     return pl.pallas_call(
         kernel,

time: 30 us -> 27.6 us (0.920)
  Pallas kernels: 28.7 us -> 26.3 us
    pallas_call x1, Pallas kernels: 28.7 us -> 26.3 us  [body(): pl.pallas_call(kernel, out_shape=pltpu.VMEM((HALF, D), BF16), in_specs=[a...]
where the time goes in v3:
time: 27.6 us; the launch traced here: 27.4 us
  Pallas kernels  26.3 us (95%)
  local copies, waits for them, and re-layouts  1.15 us (4%)
    pallas_call x1, Pallas kernels, body(): pl.pallas_call(kernel, out_shape=pltpu.VMEM((HALF, D), BF16), in_specs=[a...  26.3 us
    unnamed x1, local copies, waits for them, and re-layouts  1.15 us

profile of v3, /device:TPU:1, one launch (start us, length us, event | category | flops | bytes accessed | tf_op | source)
XLA Modules:
  0.0 27.4 jit_solution(12134824588830623528)
XLA Ops:
  0.0 26.3 %shard_map.136 = bf16[384,2048]{1,0:T(8,128)(2,1)S(1)} custom-call(bf16[768,1024]{1,0:T(8,128)(2,1)} %tok.1, bf16[2048]{0:T(1024)(128)(2,1)} %gain.1, f32[4,768]{1,0:T(4,128)} %ld.1, bf16[3,512]{1,0:T(4,128)(2,1)} %taps.1, bf16[2048,512]{1,0:T(8,128)(2,1)} %wk.1, bf16[2048,512]{1,0:T(8,128)(2,1)} %wv.1, bf16[2048,512]{1,0:T(8,128)(2,1)} %wq.1, ...), custom_call_target="tpu_custom_call" | custom-call | tf_op jit(solution)/shard_map/pallas_call | solution.py:593
  26.3 1.1 %copy.16 = bf16[384,2048]{1,0:T(8,128)(2,1)} copy(bf16[384,2048]{1,0:T(8,128)(2,1)S(1)} %shard_map.136) | data formatting | bytes 3145728

commit v4 on v3

--- a/solution.py
+++ b/solution.py
@@ -73,6 +73,8 @@
     lall[...] = jnp.zeros_like(lall)
     a2[...] = jnp.zeros_like(a2)
     b1[...] = jnp.zeros_like(b1)
+    a1[...] = jnp.zeros_like(a1)
+    b2[...] = jnp.zeros_like(b2)
 
     @pl.when(tp == 0)
     def _():
@@ -292,7 +294,7 @@
                 copy = remote(a1.at[x], a1.at[x], a1s.at[k], a1r.at[k], {"sp": row_peer[k]})
             else:
                 copy = remote(b1.at[z], b1.at[z], b1s.at[k], b1r.at[k], {"sp": col_peer[k]})
-            pl.when(True if n == 0 else z + k < 3)(copy.start)
+            pl.when((z < 3) | (x + k < 3) if n == 0 else z + k < 3)(copy.start)
             exchange.append(copy)
 
     for name in ("wk", "wv", "wq"):
@@ -353,16 +355,6 @@
         gbuf.at[:, pl.ds(ROWS, 8), :], gbuf.at[:, pl.ds(0, 8), :], hs, hr, {"sp": after}
     )
     pl.when(sp < 15)(halo.start)
-
-    @section
-    def _():
-        for n in range(2):
-            cols = slice(n * 256, n * 256 + 256)
-            qq = acc[2, :, cols] + mm(gp[...], wbuf[2, 1, :, cols])
-            for j in range(2):
-                at = slice(n * 256 + j * 128, n * 256 + j * 128 + 128)
-                qb[:, at] = rotated(qq[:, j * 128 : j * 128 + 128]).astype(BF16)
-
 
     for k in range(15):
         pl.when(lax.div(behind[k], 4) <= z)(total_copy(k).wait_recv)
@@ -412,7 +404,7 @@
             bm[k, j] = (lane_row(e_col, h) * column + lane_row(e_mine, h) * mine).astype(BF16)
     for k in range(3):
         copy = remote(bm.at[k], b2.at[x], b2s.at[k], b2r.at[k], {"sp": row_peer[k]})
-        copy.start()
+        pl.when((z > 0) | (x + k < 3))(copy.start)
         second.append(copy)
 
     for part in range(2):
@@ -423,23 +415,41 @@
             cols = slice(n * 256, n * 256 + 256)
             postb[:, cols] = full_product(5, cols)
 
-    to_end = [jnp.exp(between(i, 4)) for i in range(4)]
-    to_me = [jnp.where(i < x, jnp.exp(between(i, x)), 0.0) for i in range(4)]
-    for k in range(3):
-        exchange[k].wait_recv()
-    for j in range(2):
-        parts = [a1[i, j].astype(F32) for i in range(4)]
-        row_state = lane_row(to_end[0], j) * parts[0]
-        prefix = lane_row(to_me[0], j) * parts[0]
-        for i in range(1, 4):
-            row_state = row_state + lane_row(to_end[i], j) * parts[i]
-            prefix = prefix + lane_row(to_me[i], j) * parts[i]
-        pre[j] = prefix
-        a2[z, j] = row_state.astype(BF16)
-    for k in range(3):
-        copy = remote(a2.at[z], a2.at[z], a2s.at[k], a2r.at[k], {"sp": col_peer[k]})
-        pl.when(z + k < 3)(copy.start)
-        second.append(copy)
+
+    second += [
+        remote(a2.at[z], a2.at[z], a2s.at[k], a2r.at[k], {"sp": col_peer[k]})
+        for k in range(3)
+    ]
+
+    def pass_rows():
+        to_end = [jnp.exp(between(i, 4)) for i in range(4)]
+        to_me = [jnp.where(i < x, jnp.exp(between(i, x)), 0.0) for i in range(4)]
+        for k in range(3):
+            pl.when((z < 3) | (x > k))(exchange[k].wait_recv)
+        for j in range(2):
+            parts = [a1[i, j].astype(F32) for i in range(4)]
+            row_state = lane_row(to_end[0], j) * parts[0]
+            prefix = lane_row(to_me[0], j) * parts[0]
+            for i in range(1, 4):
+                row_state = row_state + lane_row(to_end[i], j) * parts[i]
+                prefix = prefix + lane_row(to_me[i], j) * parts[i]
+            pre[j] = prefix
+            a2[z, j] = row_state.astype(BF16)
+        for k in range(3):
+            pl.when(z + k < 3)(second[3 + k].start)
+
+    pl.when(x > 0)(pass_rows)
+
+    @section
+    def _():
+        for n in range(2):
+            cols = slice(n * 256, n * 256 + 256)
+            qq = acc[2, :, cols] + mm(gp[...], wbuf[2, 1, :, cols])
+            for j in range(2):
+                at = slice(n * 256 + j * 128, n * 256 + j * 128 + 128)
+                qb[:, at] = rotated(qq[:, j * 128 : j * 128 + 128]).astype(BF16)
+
+    pl.when(x == 0)(pass_rows)
 
     small[2].wait()
     pl.when(sp > 0)(halo.wait_recv)
@@ -460,53 +470,55 @@
     conv_send = remote(cob.at[far_rows, :], cor, cs, cr, {"tp": other})
     conv_send.start()
 
-    @section
-    def _():
-        for b in range(BLOCKS):
-            rows = slice(b * 128, b * 128 + 128)
-            for h in range(HEADS):
-                at = slice(h * 128, h * 128 + 128)
-                scores = lax.dot_general(
-                    qb[rows, at], kb[rows, at], (((1,), (1,)), ((), ())),
-                    preferred_element_type=F32,
-                )
-                both[b, h, :, :128] = (scores * fade[b, h]).astype(BF16)
-                query = qb[rows, at].astype(F32)
-                if b == 0:
-                    qs[rows, at] = (query * jnp.exp(colrep[b, h])).astype(BF16)
-                else:
-                    both[b, h, :, 128:] = (query * jnp.exp(colrep[b, h])).astype(BF16)
-                    offset = endr[h : h + 1, :]
-                    for e in range(1, b):
-                        offset = offset + block_end(e, h)
-                    qs[rows, at] = (query * jnp.exp(colrep[b, h] + offset)).astype(BF16)
-        for b in range(BLOCKS):
-            rows = slice(b * 128, b * 128 + 128)
-            for h in range(HEADS):
-                at = slice(h * 128, h * 128 + 128)
-                if b == 0:
-                    inside[rows, at] = mm(both[b, h, :, :128], vb[rows, at])
-                else:
-                    inside[rows, at] = mm(
-                        both[b, h],
-                        jnp.concatenate([vb[rows, at], starts[b, h]], axis=0),
-                    )
-
     for i in range(2):
         for part in range(2):
             wo_load(i, part).wait()
+
+    def score_block(b):
+        rows = slice(b * 128, b * 128 + 128)
+        for h in range(HEADS):
+            at = slice(h * 128, h * 128 + 128)
+            scores = lax.dot_general(
+                qb[rows, at], kb[rows, at], (((1,), (1,)), ((), ())),
+                preferred_element_type=F32,
+            )
+            both[b, h, :, :128] = (scores * fade[b, h]).astype(BF16)
+            query = qb[rows, at].astype(F32)
+            if b == 0:
+                qs[rows, at] = (query * jnp.exp(colrep[b, h])).astype(BF16)
+            else:
+                both[b, h, :, 128:] = (query * jnp.exp(colrep[b, h])).astype(BF16)
+                offset = endr[h : h + 1, :]
+                for e in range(1, b):
+                    offset = offset + block_end(e, h)
+                qs[rows, at] = (query * jnp.exp(colrep[b, h] + offset)).astype(BF16)
+
+    def value_block(b):
+        rows = slice(b * 128, b * 128 + 128)
+        for h in range(HEADS):
+            at = slice(h * 128, h * 128 + 128)
+            if b == 0:
+                inside[rows, at] = mm(both[b, h, :, :128], vb[rows, at])
+            else:
+                inside[rows, at] = mm(
+                    both[b, h],
+                    jnp.concatenate([vb[rows, at], starts[b, h]], axis=0),
+                )
+
+    @section
+    def _():
+        for n in range(8):
+            cols = slice(n * 256, n * 256 + 256)
+            oacc[:, cols] = mm(cob[own_rows, :], wob[0, 0, :, cols])
+            if n < 6:
+                score_block(n)
+            if n >= 2:
+                value_block(n - 2)
+
     conv_send.wait_recv()
 
-    @section
-    def _():
-        for n in range(8):
-            cols = slice(n * 256, n * 256 + 256)
-            oacc[:, cols] = mm(cob[own_rows, :], wob[0, 0, :, cols]) + mm(
-                cor[...], wob[0, 1, :, cols]
-            )
-
     for k in range(3):
-        second[k].wait_recv()
+        pl.when((z > 0) | (x > k))(second[k].wait_recv)
         pl.when(z > k)(second[3 + k].wait_recv)
     down = [
         jnp.where(i < z, jnp.exp(rows_between(i) + before_me), 0.0) for i in range(4)
@@ -523,24 +535,35 @@
                 state = state + b2[i, j].astype(F32)
         entry[h] = state.astype(BF16)
 
-    def across(first):
+    def across(first, i):
+        rows = pl.ds(pl.multiple_of(first + i * 128, 128), 128)
+        for h in range(HEADS):
+            at = slice(h * 128, h * 128 + 128)
+            value = inside[rows, at] + mm(qs[rows, at], entry[h])
+            level = jnp.mean(value * value, axis=1, keepdims=True)
+            retb[rows, at] = (value * lax.rsqrt(level + EPS)).astype(BF16)
+
+    @section
+    def _():
         for i in range(3):
-            rows = pl.ds(pl.multiple_of(first + i * 128, 128), 128)
-            for h in range(HEADS):
-                at = slice(h * 128, h * 128 + 128)
-                value = inside[rows, at] + mm(qs[rows, at], entry[h])
-                level = jnp.mean(value * value, axis=1, keepdims=True)
-                retb[rows, at] = (value * lax.rsqrt(level + EPS)).astype(BF16)
-
-    section(lambda: across(other * HALF))
+            across(other * HALF, i)
+
     ret_send = remote(retb.at[far_rows, :], retr, rs, rr, {"tp": other})
     ret_send.start()
-    section(lambda: across(tp * HALF))
 
     @section
     def _():
         for n in range(8):
             cols = slice(n * 256, n * 256 + 256)
+            oacc[:, cols] += mm(cor[...], wob[0, 1, :, cols])
+            if n < 3:
+                across(tp * HALF, n)
+
+
+    @section
+    def _():
+        for n in range(8):
+            cols = slice(n * 256, n * 256 + 256)
             oacc[:, cols] += mm(retb[own_rows, :], wob[1, 0, :, cols])
 
     ret_send.wait_recv()
@@ -551,10 +574,12 @@
             cols = slice(n * 256, n * 256 + 256)
             out[:, cols] = (oacc[:, cols] + mm(retr[...], wob[1, 1, :, cols])).astype(BF16)
 
-    for copy in [pack_send, conv_send, ret_send] + tok_send + exchange[:3] + second[:3]:
+    for copy in [pack_send, conv_send, ret_send] + tok_send:
         copy.wait_send()
     pl.when(sp < 15)(halo.wait_send)
     for k in range(3):
+        pl.when((z < 3) | (x + k < 3))(exchange[k].wait_send)
+        pl.when((z > 0) | (x + k < 3))(second[k].wait_send)
         pl.when(z + k < 3)(exchange[3 + k].wait_send)
         pl.when(z + k < 3)(second[3 + k].wait_send)
     for k in range(15):

time: 27.6 us -> 26.2 us (0.949)
  Pallas kernels: 26.3 us -> 24.9 us
    pallas_call x1, Pallas kernels: 26.3 us -> 24.9 us  [body(): pl.pallas_call(kernel, out_shape=pltpu.VMEM((HALF, D), BF16), in_specs=[a...]
where the time goes in v4:
time: 26.2 us; the launch traced here: 26.1 us
  Pallas kernels  24.9 us (95%)
  local copies, waits for them, and re-layouts  1.15 us (4%)
    pallas_call x1, Pallas kernels, body(): pl.pallas_call(kernel, out_shape=pltpu.VMEM((HALF, D), BF16), in_specs=[a...  24.9 us
    unnamed x1, local copies, waits for them, and re-layouts  1.15 us

profile of v4, /device:TPU:1, one launch (start us, length us, event | category | flops | bytes accessed | tf_op | source)
XLA Modules:
  0.0 26.1 jit_solution(15637079054651594651)
XLA Ops:
  0.0 24.9 %shard_map.136 = bf16[384,2048]{1,0:T(8,128)(2,1)S(1)} custom-call(bf16[768,1024]{1,0:T(8,128)(2,1)} %tok.1, bf16[2048]{0:T(1024)(128)(2,1)} %gain.1, f32[4,768]{1,0:T(4,128)} %ld.1, bf16[3,512]{1,0:T(4,128)(2,1)} %taps.1, bf16[2048,512]{1,0:T(8,128)(2,1)} %wk.1, bf16[2048,512]{1,0:T(8,128)(2,1)} %wv.1, bf16[2048,512]{1,0:T(8,128)(2,1)} %wq.1, ...), custom_call_target="tpu_custom_call" | custom-call | tf_op jit(solution)/shard_map/pallas_call | solution.py:618
  24.9 1.1 %copy.16 = bf16[384,2048]{1,0:T(8,128)(2,1)} copy(bf16[384,2048]{1,0:T(8,128)(2,1)S(1)} %shard_map.136) | data formatting | bytes 3145728

commit v5 on v4

--- a/solution.py
+++ b/solution.py
@@ -53,7 +53,7 @@
     xo, go, gp, wbuf, wob, acc, kb, vb, qb, cib, postb, gbuf, cob, cor,
     retb, retr, inside, starts, oacc, ssb, pack, pack_far, rot_c, rot_s,
     tabv, basev, gainv, ldv, tapv, ldp, cumr, colrep, lall,
-    a1, a2, b1, b2, bm, pre, fade, tails, cumc, endr, qs, entry, both,
+    a1, a2, b1, b2, bm, pre, fade, tails, cumc, endr, qs, entry, both, downv,
     sem_tok, sem_small, sem_w, sem_wo,
     ts, tr, ls, lr, a1s, a1r, a2s, a2r, b1s, b1r, b2s, b2r,
     hs, hr, cs, cr, rs, rr, ps, pr, met,
@@ -68,17 +68,6 @@
     after = lax.rem(sp + 1, 16)
     ahead = [lax.rem(sp + k, 16) for k in range(1, 16)]
     behind = [lax.rem(sp + 16 - k, 16) for k in range(1, 16)]
-
-    barrier = pltpu.get_barrier_semaphore()
-    lall[...] = jnp.zeros_like(lall)
-    a2[...] = jnp.zeros_like(a2)
-    b1[...] = jnp.zeros_like(b1)
-    a1[...] = jnp.zeros_like(a1)
-    b2[...] = jnp.zeros_like(b2)
-
-    @pl.when(tp == 0)
-    def _():
-        pl.semaphore_signal(barrier, inc=1, device_id={"tp": 1}, device_id_type=MESH)
 
     def remote(src, dst, send, recv, where):
         return pltpu.make_async_remote_copy(
@@ -122,15 +111,37 @@
             (woc, wor)[i].at[rows, :], wob.at[i, part], sem_wo.at[i * 2 + part]
         )
 
+    for copy in tok_load:
+        copy.start()
     small[0].start()
     small[1].start()
-    for copy in tok_load:
-        copy.start()
     w_load("wk", 0).start()
     w_load("wv", 0).start()
     small[4].start()
     small[3].start()
     small[2].start()
+
+    barrier = pltpu.get_barrier_semaphore()
+    lall[...] = jnp.zeros_like(lall)
+    a2[...] = jnp.zeros_like(a2)
+    b1[...] = jnp.zeros_like(b1)
+    a1[...] = jnp.zeros_like(a1)
+    b2[...] = jnp.zeros_like(b2)
+
+    @pl.when(tp == 0)
+    def _():
+        pl.semaphore_signal(barrier, inc=1, device_id={"tp": 1}, device_id_type=MESH)
+
+    @pl.when(tp == 1)
+    def _():
+        pl.semaphore_wait(barrier, 1)
+        pl.semaphore_signal(met, inc=1, device_id={"tp": 0}, device_id_type=MESH)
+
+    @pl.when(tp == 0)
+    def _():
+        pl.semaphore_wait(met, 1)
+        for peer in ahead:
+            pl.semaphore_signal(barrier, inc=1, device_id={"sp": peer}, device_id_type=MESH)
 
     lane = lax.broadcasted_iota(jnp.int32, (SPAN, SPAN), 1)
     packed = jnp.zeros((SPAN, SPAN), F32)
@@ -144,17 +155,6 @@
         ssb[rows, :] = spread
         packed = jnp.where(lane == i, spread, packed)
     pack[...] = packed
-
-    @pl.when(tp == 1)
-    def _():
-        pl.semaphore_wait(barrier, 1)
-        pl.semaphore_signal(met, inc=1, device_id={"tp": 0}, device_id_type=MESH)
-
-    @pl.when(tp == 0)
-    def _():
-        pl.semaphore_wait(met, 1)
-        for peer in ahead:
-            pl.semaphore_signal(barrier, inc=1, device_id={"sp": peer}, device_id_type=MESH)
 
     pack_send = remote(pack, pack_far, ps, pr, {"tp": other})
     pack_send.start()
@@ -259,12 +259,15 @@
 
     exchange = []
 
-    def key_value(n):
+    def keys_of(n):
         cols = slice(n * 256, n * 256 + 256)
         kk = acc[0, :, cols] + mm(gp[...], wbuf[0, 1, :, cols])
         for j in range(2):
             at = slice(n * 256 + j * 128, n * 256 + j * 128 + 128)
             kb[:, at] = (rotated(kk[:, j * 128 : j * 128 + 128]) * KEY_SCALE).astype(BF16)
+
+    def values_of(n):
+        cols = slice(n * 256, n * 256 + 256)
         vv = acc[1, :, cols] + mm(gp[...], wbuf[1, 1, :, cols])
         vb[:, cols] = vv.astype(BF16)
 
@@ -288,22 +291,26 @@
                     whole = jnp.exp(block_end(b, h)) * whole + fresh
             slot[j] = whole.astype(BF16)
 
+    def start_along_row(copies, always):
+        pl.when((x == 2) & always)(copies[1].start)
+        for k in range(3):
+            wanted = always | (x + k < 3)
+            pl.when(wanted & (x != 2) if k == 1 else wanted)(copies[k].start)
+
     def send_states(n):
         for k in range(3):
             if n == 0:
                 copy = remote(a1.at[x], a1.at[x], a1s.at[k], a1r.at[k], {"sp": row_peer[k]})
             else:
                 copy = remote(b1.at[z], b1.at[z], b1s.at[k], b1r.at[k], {"sp": col_peer[k]})
-            pl.when((z < 3) | (x + k < 3) if n == 0 else z + k < 3)(copy.start)
             exchange.append(copy)
+            if n == 1:
+                pl.when(z + k < 3)(copy.start)
+        if n == 0:
+            start_along_row(exchange, z < 3)
 
     for name in ("wk", "wv", "wq"):
         w_load(name, 1).wait()
-    @section
-    def _():
-        key_value(0)
-        key_value(1)
-
     @pl.when(tp == 0)
     def _():
         pl.semaphore_wait(barrier, 15)
@@ -318,6 +325,13 @@
 
     for k in range(15):
         pl.when(lax.div(ahead[k], 4) >= z)(total_copy(k).start)
+
+    @section
+    def _():
+        keys_of(0)
+        keys_of(1)
+        values_of(0)
+        values_of(1)
 
     @section
     def _():
@@ -404,8 +418,8 @@
             bm[k, j] = (lane_row(e_col, h) * column + lane_row(e_mine, h) * mine).astype(BF16)
     for k in range(3):
         copy = remote(bm.at[k], b2.at[x], b2s.at[k], b2r.at[k], {"sp": row_peer[k]})
-        pl.when((z > 0) | (x + k < 3))(copy.start)
         second.append(copy)
+    start_along_row(second, z > 0)
 
     for part in range(2):
         w_load("wcq", part).wait()
@@ -413,7 +427,11 @@
     def _():
         for n in range(2):
             cols = slice(n * 256, n * 256 + 256)
-            postb[:, cols] = full_product(5, cols)
+            qq = acc[2, :, cols] + mm(gp[...], wbuf[2, 1, :, cols])
+            for j in range(2):
+                at = slice(n * 256 + j * 128, n * 256 + j * 128 + 128)
+                qb[:, at] = rotated(qq[:, j * 128 : j * 128 + 128]).astype(BF16)
+        postb[:, 0:256] = full_product(5, slice(0, 256))
 
 
     second += [
@@ -442,14 +460,11 @@
 
     @section
     def _():
-        for n in range(2):
-            cols = slice(n * 256, n * 256 + 256)
-            qq = acc[2, :, cols] + mm(gp[...], wbuf[2, 1, :, cols])
-            for j in range(2):
-                at = slice(n * 256 + j * 128, n * 256 + j * 128 + 128)
-                qb[:, at] = rotated(qq[:, j * 128 : j * 128 + 128]).astype(BF16)
+        postb[:, 256:512] = full_product(5, slice(256, 512))
 
     pl.when(x == 0)(pass_rows)
+    for i in range(4):
+        downv[i] = jnp.where(i < z, jnp.exp(rows_between(i) + before_me), 0.0)
 
     small[2].wait()
     pl.when(sp > 0)(halo.wait_recv)
@@ -517,12 +532,18 @@
 
     conv_send.wait_recv()
 
+    for k in range(15):
+        pl.when(lax.div(ahead[k], 4) >= z)(total_copy(k).wait_send)
+    for k in range(3):
+        pl.when((z < 3) | (x + k < 3))(exchange[k].wait_send)
+        pl.when(z + k < 3)(exchange[3 + k].wait_send)
+    pl.when(sp < 15)(halo.wait_send)
+    for copy in [pack_send] + tok_send:
+        copy.wait_send()
     for k in range(3):
         pl.when((z > 0) | (x > k))(second[k].wait_recv)
         pl.when(z > k)(second[3 + k].wait_recv)
-    down = [
-        jnp.where(i < z, jnp.exp(rows_between(i) + before_me), 0.0) for i in range(4)
-    ]
+    down = [downv[i] for i in range(4)]
     for h in range(HEADS):
         j = h % 2
         if h < 2:
@@ -574,16 +595,11 @@
             cols = slice(n * 256, n * 256 + 256)
             out[:, cols] = (oacc[:, cols] + mm(retr[...], wob[1, 1, :, cols])).astype(BF16)
 
-    for copy in [pack_send, conv_send, ret_send] + tok_send:
+    for copy in [conv_send, ret_send]:
         copy.wait_send()
-    pl.when(sp < 15)(halo.wait_send)
     for k in range(3):
-        pl.when((z < 3) | (x + k < 3))(exchange[k].wait_send)
         pl.when((z > 0) | (x + k < 3))(second[k].wait_send)
-        pl.when(z + k < 3)(exchange[3 + k].wait_send)
         pl.when(z + k < 3)(second[3 + k].wait_send)
-    for k in range(15):
-        pl.when(lax.div(ahead[k], 4) >= z)(total_copy(k).wait_send)
 
 
 def body(
@@ -611,7 +627,7 @@
         v((3, 2, 128, 128), BF16), v((2, 128, 128), F32),
         v((BLOCKS, HEADS, 128, 128), F32), v((BLOCKS, HEADS, 128, 128), F32),
         v((128, 128), F32), v((128, 128), F32), v((ROWS, NW), BF16), v((HEADS, 128, 128), BF16),
-        v((BLOCKS, HEADS, 128, 256), BF16),
+        v((BLOCKS, HEADS, 128, 256), BF16), v((4, 8, 128), F32),
         dma((3,)), dma((5,)), dma((12,)), dma((4,)),
     ] + [dma((3,))] * 2 + [dma((15,))] * 2 + [dma((3,))] * 8 + [dma] * 8 + [pltpu.SemaphoreType.REGULAR]
     anywhere = pl.BlockSpec(memory_space=pltpu.HBM)

time: 26.2 us -> 25.8 us (0.985)
  Pallas kernels: 24.9 us -> 24.5 us
    pallas_call x1, Pallas kernels: 24.9 us -> 24.5 us  [body(): pl.pallas_call(kernel, out_shape=pltpu.VMEM((HALF, D), BF16), in_specs=[a...]
where the time goes in v5:
time: 25.8 us; the launch traced here: 25.6 us
  Pallas kernels  24.5 us (95%)
  local copies, waits for them, and re-layouts  1.15 us (4%)
    pallas_call x1, Pallas kernels, body(): pl.pallas_call(kernel, out_shape=pltpu.VMEM((HALF, D), BF16), in_specs=[a...  24.5 us
    unnamed x1, local copies, waits for them, and re-layouts  1.15 us

profile of v5, /device:TPU:1, one launch (start us, length us, event | category | flops | bytes accessed | tf_op | source)
XLA Modules:
  0.0 25.6 jit_solution(6321337068597073107)
XLA Ops:
  0.0 24.5 %shard_map.136 = bf16[384,2048]{1,0:T(8,128)(2,1)S(1)} custom-call(bf16[768,1024]{1,0:T(8,128)(2,1)} %tok.1, bf16[2048]{0:T(1024)(128)(2,1)} %gain.1, f32[4,768]{1,0:T(4,128)} %ld.1, bf16[3,512]{1,0:T(4,128)(2,1)} %taps.1, bf16[2048,512]{1,0:T(8,128)(2,1)} %wk.1, bf16[2048,512]{1,0:T(8,128)(2,1)} %wv.1, bf16[2048,512]{1,0:T(8,128)(2,1)} %wq.1, ...), custom_call_target="tpu_custom_call" | custom-call | tf_op jit(solution)/shard_map/pallas_call | solution.py:634
  24.5 1.1 %copy.16 = bf16[384,2048]{1,0:T(8,128)(2,1)} copy(bf16[384,2048]{1,0:T(8,128)(2,1)S(1)} %shard_map.136) | data formatting | bytes 3145728

commit v6 on v5

--- a/solution.py
+++ b/solution.py
@@ -51,7 +51,7 @@
     tok, gain, ld, taps, wk, wv, wq, wci, wcp, wcq, woc, wor, tabs, bases,
     out,
     xo, go, gp, wbuf, wob, acc, kb, vb, qb, cib, postb, gbuf, cob, cor,
-    retb, retr, inside, starts, oacc, ssb, pack, pack_far, rot_c, rot_s,
+    retb, retr, inside, starts, oacc, ssb, pack, pack_far, rot_c, rot_s, key_c, key_s,
     tabv, basev, gainv, ldv, tapv, ldp, cumr, colrep, lall,
     a1, a2, b1, b2, bm, pre, fade, tails, cumc, endr, qs, entry, both, downv,
     sem_tok, sem_small, sem_w, sem_wo,
@@ -240,6 +240,8 @@
             base_s = basev[b + 8 : b + 9, :]
             rot_c[rows, :] = base_c * tabv[0] - base_s * tabv[1]
             rot_s[rows, :] = base_s * tabv[2] + base_c * tabv[3]
+            key_c[rows, :] = rot_c[rows, :] * KEY_SCALE
+            key_s[rows, :] = rot_s[rows, :] * KEY_SCALE
         near_product(1)
         for b in range(BLOCKS):
             for h in range(HEADS):
@@ -248,7 +250,7 @@
                 colrep[b, h] = column
                 gap = column - cumr[i : i + 1, :]
                 fade[b, h] = jnp.where(lower, jnp.exp(jnp.minimum(gap, 0.0)), 0.0)
-                tails[b, h] = jnp.exp(block_end(b, h) - column)
+                tails[b, h] = jnp.exp(block_end(b, h) - column).astype(BF16)
         near_product(2)
 
     for copy in tok_send:
@@ -264,7 +266,8 @@
         kk = acc[0, :, cols] + mm(gp[...], wbuf[0, 1, :, cols])
         for j in range(2):
             at = slice(n * 256 + j * 128, n * 256 + j * 128 + 128)
-            kb[:, at] = (rotated(kk[:, j * 128 : j * 128 + 128]) * KEY_SCALE).astype(BF16)
+            piece = kk[:, j * 128 : j * 128 + 128]
+            kb[:, at] = (piece * key_c[...] + pltpu.roll(piece, 64, axis=1) * key_s[...]).astype(BF16)
 
     def values_of(n):
         cols = slice(n * 256, n * 256 + 256)
@@ -279,7 +282,7 @@
             whole = None
             for b in range(BLOCKS):
                 rows = slice(b * 128, b * 128 + 128)
-                weighted = (vb[rows, at].astype(F32) * tails[b, h]).astype(BF16)
+                weighted = vb[rows, at] * tails[b, h]
                 fresh = lax.dot_general(
                     kb[rows, at], weighted, (((0,), (0,)), ((), ())),
                     preferred_element_type=F32,
@@ -456,13 +459,12 @@
         for k in range(3):
             pl.when(z + k < 3)(second[3 + k].start)
 
-    pl.when(x > 0)(pass_rows)
+    pass_rows()
 
     @section
     def _():
         postb[:, 256:512] = full_product(5, slice(256, 512))
 
-    pl.when(x == 0)(pass_rows)
     for i in range(4):
         downv[i] = jnp.where(i < z, jnp.exp(rows_between(i) + before_me), 0.0)
 
@@ -477,8 +479,8 @@
     def _():
         for c in range(4):
             at = slice(c * 128, c * 128 + 128)
-            summed = jnp.zeros((ROWS, 128), F32)
-            for i in range(3):
+            summed = tapv[0:1, at].astype(F32) * gbuf[c, 6 : 6 + ROWS, :]
+            for i in range(1, 3):
                 summed = summed + tapv[i : i + 1, at].astype(F32) * gbuf[c, 6 + i : 6 + i + ROWS, :]
             cob[:, at] = (postb[:, at].astype(F32) * summed).astype(BF16)
 
@@ -618,14 +620,14 @@
         v((ROWS, NW), F32),
         v((BLOCKS, HEADS, 128, 128), BF16), v((HALF, D), F32),
         v((ROWS, 128), F32), v((128, 128), F32), v((128, 128), F32),
-        v((ROWS, 128), F32), v((ROWS, 128), F32),
+        v((ROWS, 128), F32), v((ROWS, 128), F32), v((ROWS, 128), F32), v((ROWS, 128), F32),
         v((4, 128, 128), F32), v((16, 128), F32), v((D,), BF16), v((HEADS, ROWS), F32),
         v((3, NW), BF16), v((128, 128), F32), v((128, 128), F32),
         v((BLOCKS, HEADS, 128, 128), F32), v((16, 8, 128), F32),
         v((4, 2, 128, 128), BF16), v((4, 2, 128, 128), BF16),
         v((4, 2, 128, 128), BF16), v((4, 2, 128, 128), BF16),
         v((3, 2, 128, 128), BF16), v((2, 128, 128), F32),
-        v((BLOCKS, HEADS, 128, 128), F32), v((BLOCKS, HEADS, 128, 128), F32),
+        v((BLOCKS, HEADS, 128, 128), F32), v((BLOCKS, HEADS, 128, 128), BF16),
         v((128, 128), F32), v((128, 128), F32), v((ROWS, NW), BF16), v((HEADS, 128, 128), BF16),
         v((BLOCKS, HEADS, 128, 256), BF16), v((4, 8, 128), F32),
         dma((3,)), dma((5,)), dma((12,)), dma((4,)),

time: 25.8 us -> 25.8 us (level)
  no operation moved by 1% of the time
where the time goes in v6:
time: 25.8 us; the launch traced here: 25.6 us
  Pallas kernels  24.5 us (95%)
  local copies, waits for them, and re-layouts  1.15 us (4%)
    pallas_call x1, Pallas kernels, body(): pl.pallas_call(kernel, out_shape=pltpu.VMEM((HALF, D), BF16), in_specs=[a...  24.5 us
    unnamed x1, local copies, waits for them, and re-layouts  1.15 us

profile of v6, /device:TPU:1, one launch (start us, length us, event | category | flops | bytes accessed | tf_op | source)
XLA Modules:
  0.0 25.6 jit_solution(6047896713517693115)
XLA Ops:
  0.0 24.5 %shard_map.136 = bf16[384,2048]{1,0:T(8,128)(2,1)S(1)} custom-call(bf16[768,1024]{1,0:T(8,128)(2,1)} %tok.1, bf16[2048]{0:T(1024)(128)(2,1)} %gain.1, f32[4,768]{1,0:T(4,128)} %ld.1, bf16[3,512]{1,0:T(4,128)(2,1)} %taps.1, bf16[2048,512]{1,0:T(8,128)(2,1)} %wk.1, bf16[2048,512]{1,0:T(8,128)(2,1)} %wv.1, bf16[2048,512]{1,0:T(8,128)(2,1)} %wq.1, ...), custom_call_target="tpu_custom_call" | custom-call | tf_op jit(solution)/shard_map/pallas_call | solution.py:636
  24.5 1.1 %copy.16 = bf16[384,2048]{1,0:T(8,128)(2,1)} copy(bf16[384,2048]{1,0:T(8,128)(2,1)S(1)} %shard_map.136) | data formatting | bytes 3145728

commit v7 on v6

--- a/solution.py
+++ b/solution.py
@@ -259,7 +259,7 @@
     def rotated(value):
         return value * rot_c[...] + pltpu.roll(value, 64, axis=1) * rot_s[...]
 
-    exchange = []
+    exchange = [None] * 6
 
     def keys_of(n):
         cols = slice(n * 256, n * 256 + 256)
@@ -306,7 +306,7 @@
                 copy = remote(a1.at[x], a1.at[x], a1s.at[k], a1r.at[k], {"sp": row_peer[k]})
             else:
                 copy = remote(b1.at[z], b1.at[z], b1s.at[k], b1r.at[k], {"sp": col_peer[k]})
-            exchange.append(copy)
+            exchange[3 * n + k] = copy
             if n == 1:
                 pl.when(z + k < 3)(copy.start)
         if n == 0:
@@ -324,7 +324,11 @@
         pl.semaphore_wait(met, 1)
 
     def total_copy(k):
-        return remote(lall.at[sp], lall.at[sp], ls.at[k], lr.at[k], {"sp": ahead[k]})
+        return remote(lall.at[sp], lall.at[sp], ls, lr, {"sp": ahead[k]})
+
+    def all_totals(count):
+        part = lall.at[pl.ds(0, count)]
+        return remote(part, part, ls, lr, {"sp": ahead[0]})
 
     for k in range(15):
         pl.when(lax.div(ahead[k], 4) >= z)(total_copy(k).start)
@@ -341,8 +345,8 @@
         fresh_states(0)
         fresh_states(1)
 
+    send_states(1)
     send_states(0)
-    send_states(1)
 
     for name in ("wci", "wcp"):
         for part in range(2):
@@ -373,8 +377,8 @@
     )
     pl.when(sp < 15)(halo.start)
 
-    for k in range(15):
-        pl.when(lax.div(behind[k], 4) <= z)(total_copy(k).wait_recv)
+    for i in range(4):
+        pl.when(z == i)(all_totals(4 * i + 3).wait_recv)
     totals = [[lall[4 * i + j] for j in range(4)] for i in range(4)]
     line = [lall[4 * z + j] for j in range(4)]
 
@@ -534,8 +538,8 @@
 
     conv_send.wait_recv()
 
-    for k in range(15):
-        pl.when(lax.div(ahead[k], 4) >= z)(total_copy(k).wait_send)
+    for i in range(4):
+        pl.when(z == i)(all_totals(15 - 4 * i).wait_send)
     for k in range(3):
         pl.when((z < 3) | (x + k < 3))(exchange[k].wait_send)
         pl.when(z + k < 3)(exchange[3 + k].wait_send)
@@ -631,7 +635,7 @@
         v((128, 128), F32), v((128, 128), F32), v((ROWS, NW), BF16), v((HEADS, 128, 128), BF16),
         v((BLOCKS, HEADS, 128, 256), BF16), v((4, 8, 128), F32),
         dma((3,)), dma((5,)), dma((12,)), dma((4,)),
-    ] + [dma((3,))] * 2 + [dma((15,))] * 2 + [dma((3,))] * 8 + [dma] * 8 + [pltpu.SemaphoreType.REGULAR]
+    ] + [dma((3,))] * 2 + [dma] * 2 + [dma((3,))] * 8 + [dma] * 8 + [pltpu.SemaphoreType.REGULAR]
     anywhere = pl.BlockSpec(memory_space=pltpu.HBM)
     return pl.pallas_call(
         kernel,

time: 25.8 us -> 25.5 us (0.988)
  Pallas kernels: 24.5 us -> 24.2 us
    pallas_call x1, Pallas kernels: 24.5 us -> 24.2 us  [body(): pl.pallas_call(kernel, out_shape=pltpu.VMEM((HALF, D), BF16), in_specs=[a...]
where the time goes in v7:
time: 25.5 us; the launch traced here: 25.3 us
  Pallas kernels  24.2 us (95%)
  local copies, waits for them, and re-layouts  1.15 us (5%)
    pallas_call x1, Pallas kernels, body(): pl.pallas_call(kernel, out_shape=pltpu.VMEM((HALF, D), BF16), in_specs=[a...  24.2 us
    unnamed x1, local copies, waits for them, and re-layouts  1.15 us

profile of v7, /device:TPU:1, one launch (start us, length us, event | category | flops | bytes accessed | tf_op | source)
XLA Modules:
  0.0 25.3 jit_solution(14492600464691115989)
XLA Ops:
  0.0 24.2 %shard_map.136 = bf16[384,2048]{1,0:T(8,128)(2,1)S(1)} custom-call(bf16[768,1024]{1,0:T(8,128)(2,1)} %tok.1, bf16[2048]{0:T(1024)(128)(2,1)} %gain.1, f32[4,768]{1,0:T(4,128)} %ld.1, bf16[3,512]{1,0:T(4,128)(2,1)} %taps.1, bf16[2048,512]{1,0:T(8,128)(2,1)} %wk.1, bf16[2048,512]{1,0:T(8,128)(2,1)} %wv.1, bf16[2048,512]{1,0:T(8,128)(2,1)} %wq.1, ...), custom_call_target="tpu_custom_call" | custom-call | tf_op jit(solution)/shard_map/pallas_call | solution.py:640
  24.2 1.1 %copy.16 = bf16[384,2048]{1,0:T(8,128)(2,1)} copy(bf16[384,2048]{1,0:T(8,128)(2,1)S(1)} %shard_map.136) | data formatting | bytes 3145728
